TPU v7x, 32 devices: a whole 2x2x4 slice. The times are simulated.
32 devices in a mesh: sp: 8 (over z, x), tp: 4 (over y, core).
Axes of the slice: x: 2, y: 2, z: 4, core: 2. Of those that a mesh axis runs over, the one named last changes fastest.
Arguments:
- tokens: bfloat16 [8192, 4096], P('sp'), may hold values from -6 to 6
- input_norm_scale: bfloat16 [4096], replicated, may hold values from 0.099609375 to 1.8984375
- mean_input_weight: bfloat16 [4096, 2048], P('sp', 'tp'), may hold values from -0.09375 to 0.09375
- query_matrix: bfloat16 [4096, 2048], P('sp', 'tp'), may hold values from -0.09375 to 0.09375
- key_matrix: bfloat16 [4096, 2048], P('sp', 'tp'), may hold values from -0.09375 to 0.09375
- value_matrix: bfloat16 [4096, 2048], P('sp', 'tp'), may hold values from -0.09375 to 0.09375
- strength_weight: bfloat16 [4096, 16], P('sp', 'tp'), may hold values from -0.09375 to 0.09375
- decay_input_weight: bfloat16 [4096, 16], P('sp', 'tp'), may hold values from -0.25 to 0.25
- causal_filter_weight: bfloat16 [4, 3, 2048], replicated, may hold values from -3 to 3
- head_decay_logrates: float32 [16], replicated, may hold values from -13.2 to -2.9
- decay_input_shift: float32 [16], replicated, may hold values from -1 to 1
- strength_shift: float32 [16], replicated, may hold values from -5 to -3
- decay_spike: float32 [8192, 16], P('sp', 'tp'), may hold values from -1.3 to 0
- head_norm_scale: bfloat16 [128], replicated, may hold values from 0.099609375 to 1.8984375
- group_mixing_weight: bfloat16 [16, 128, 128], replicated, may hold values from -0.5 to 0.5
- mean_channel_scale: bfloat16 [2048], replicated, may hold values from 0.099609375 to 1.8984375
- mean_output_weight: bfloat16 [2048, 4096], P('tp', 'sp'), may hold values from -0.09375 to 0.09375
- delta_output_weight: bfloat16 [2048, 4096], P('tp', 'sp'), may hold values from -0.09375 to 0.09375
Outputs:
- mixed_out: bfloat16 [8192, 4096], P(('sp', 'tp'))
All inputs are finite; a program needn't handle non-finite values.
Results may differ from a plain program's by a relative error of at most 0.015.
Values may be sent and summed in bfloat16 or wider, within the bound.
A program may use at most 128 MiB of HBM per device.

v0:
```python
import jax
import jax.numpy as jnp
from jax import lax
from jax.experimental import pallas as pl
from jax.experimental.pallas import tpu as pltpu
from jax.sharding import PartitionSpec as P

GROUP_DIM = 128
HEAD_DIM = 128
CONV = 4
BLOCK = 64


EPSILON = 1e-06


def shifted_2(block, axis, distance):
    devices = range(lax.axis_size(axis))
    route = [(i - distance, i) for i in devices if i - distance in devices]
    return lax.ppermute(block, axis, route)


def scale_rows(values, gain_vec):
    squares = jnp.mean(values * values, axis=-1, keepdims=True)
    return values * lax.rsqrt(squares + EPSILON) * gain_vec.astype(jnp.float32)


def pool_means(previous, current, group_ids, positions):
    pool_reach = 15
    rows_out = current.shape[0]
    extended = jnp.concatenate([previous, current], axis=0).astype(jnp.float32)
    window_size = jnp.left_shift(jnp.int32(2), group_ids % 4)
    windowed = jnp.zeros(current.shape, jnp.float32)
    for lag_rows in range(pool_reach + 1):
        shifted = extended[pool_reach - lag_rows : pool_reach - lag_rows + rows_out]
        windowed = windowed + jnp.where(lag_rows < window_size[None, :], shifted, 0.0)
    counts = jnp.minimum(positions[:, None] + 1, window_size[None, :]).astype(jnp.float32)
    return (windowed / counts - extended[pool_reach:]).astype(jnp.bfloat16)


BF16 = jnp.bfloat16
F32 = jnp.float32
HALO = 8


def dot(left, right):
    return jnp.dot(left.astype(BF16), right.astype(BF16), preferred_element_type=F32)


def dot_nt(left, right):
    return lax.dot_general(
        left.astype(BF16),
        right.astype(BF16),
        (((1,), (1,)), ((), ())),
        preferred_element_type=F32,
    )


def dot_tn(left, right):
    return lax.dot_general(
        left.astype(BF16),
        right.astype(BF16),
        (((0,), (0,)), ((), ())),
        preferred_element_type=F32,
    )


def unit_rows(values):
    return values * lax.rsqrt(jnp.sum(values * values, axis=-1, keepdims=True) + EPSILON)


def delta_kernel(heads, depth, chunk, *refs):
    (q_ref, k_ref, v_ref, hq_ref, hk_ref, hv_ref, tap_ref, beta_ref, decay_ref) = refs[:9]
    out_ref, eff_ref, state_ref, carry, halo = refs[9:]
    step = pl.program_id(0)
    width = heads * depth
    row = lax.broadcasted_iota(jnp.int32, (chunk, chunk), 0)
    col = lax.broadcasted_iota(jnp.int32, (chunk, chunk), 1)
    causal = row >= col
    strict = row > col
    eye = jnp.where(row == col, 1.0, 0.0)
    lane = lax.broadcasted_iota(jnp.int32, (depth, 2 * depth), 1)
    sub = lax.broadcasted_iota(jnp.int32, (depth, 2 * depth), 0)

    @pl.when(step == 0)
    def _():
        for h in range(heads):
            carry[h] = jnp.where(lane == sub + depth, 1.0, 0.0)
        halo[0] = hq_ref[...].astype(F32)
        halo[1] = hk_ref[...].astype(F32)
        halo[2] = hv_ref[...].astype(F32)

    convolved = []
    for r, ref in enumerate((q_ref, k_ref, v_ref)):
        current = ref[...].astype(F32)
        extended = jnp.concatenate([halo[r], current], axis=0)
        halo[r] = current[chunk - HALO :]
        total = jnp.zeros((chunk, width), F32)
        for i in range(CONV):
            start = HALO - (CONV - 1) + i
            taps = tap_ref[i, r : r + 1, :].astype(F32)
            total = total + taps * extended[start : start + chunk]
        convolved.append(total / (1.0 + jnp.exp(-total)))
    tri = jnp.where(causal, 1.0, 0.0)
    decay = decay_ref[...]
    cum_cols = jnp.dot(tri, decay, preferred_element_type=F32, precision=lax.Precision.HIGHEST)
    cum_rows = lax.dot_general(
        decay,
        tri,
        (((0,), (1,)), ((), ())),
        preferred_element_type=F32,
        precision=lax.Precision.HIGHEST,
    )
    base = min(16, chunk)
    hs = range(heads)
    q = [unit_rows(convolved[0][:, h * depth : (h + 1) * depth]) * depth ** (-0.5) for h in hs]
    k = [unit_rows(convolved[1][:, h * depth : (h + 1) * depth]) for h in hs]
    v = [convolved[2][:, h * depth : (h + 1) * depth] for h in hs]
    cum = [cum_cols[:, h : h + 1] for h in hs]
    last = [cum_cols[chunk - 1 : chunk, h : h + 1] for h in hs]
    beta = [beta_ref[:, h : h + 1] for h in hs]
    weights = [
        jnp.where(causal, jnp.exp(jnp.where(causal, cum[h] - cum_rows[h : h + 1, :], 0.0)), 0.0)
        for h in hs
    ]
    kb = [k[h] * beta[h] for h in hs]
    lower = [jnp.where(strict, dot_nt(kb[h], k[h]) * weights[h], 0.0) for h in hs]
    power = [jnp.where(row // base == col // base, lower[h], 0.0) for h in hs]
    inverse = [eye - power[h] for h in hs]
    reach = 2
    while reach < base:
        power = [dot(power[h], power[h]) for h in hs]
        inverse = [inverse[h] + dot(inverse[h], power[h]) for h in hs]
        reach *= 2
    size = base
    while size < chunk:
        pair = (row // (2 * size) == col // (2 * size)) & (row // size != col // size)
        right = [dot(jnp.where(pair, lower[h], 0.0), inverse[h]) for h in hs]
        inverse = [inverse[h] - dot(inverse[h], right[h]) for h in hs]
        size *= 2
    grow = [jnp.exp(cum[h]) for h in hs]
    sides = [jnp.concatenate([v[h] * beta[h], kb[h] * grow[h]], axis=1) for h in hs]
    solved = [dot(inverse[h], sides[h]) for h in hs]
    scores = [dot_nt(q[h], k[h]) * weights[h] for h in hs]
    kd = [k[h] * jnp.exp(last[h] - cum[h]) for h in hs]
    zeros = jnp.zeros((chunk, depth), F32)
    state = [carry[h] for h in hs]
    fresh = [
        jnp.concatenate([solved[h][:, :depth], zeros], axis=1) - dot(solved[h][:, depth:], state[h])
        for h in hs
    ]
    outs = [dot(q[h] * grow[h], state[h]) + dot(scores[h], fresh[h]) for h in hs]
    for h in hs:
        carry[h] = state[h] * jnp.exp(last[h]) + dot_tn(kd[h], fresh[h])
        out_ref[:, h * depth : (h + 1) * depth] = outs[h][:, :depth]
        eff_ref[:, h * depth : (h + 1) * depth] = outs[h][:, depth:].astype(BF16)
        state_ref[h] = carry[h]


def delta_pass(q, k, v, hq, hk, hv, taps, beta, decay, depth):
    rows, width = q.shape
    heads = beta.shape[1]
    chunk = min(128, rows)
    whole = lambda shape: pl.BlockSpec(shape, lambda i: (0,) * len(shape))
    tile = pl.BlockSpec((chunk, width), lambda i: (i, 0))
    slim = pl.BlockSpec((chunk, heads), lambda i: (i, 0))
    return pl.pallas_call(
        lambda *refs: delta_kernel(heads, depth, chunk, *refs),
        grid=(rows // chunk,),
        in_specs=[tile] * 3 + [whole(hq.shape)] * 3 + [whole(taps.shape), slim, slim],
        out_specs=[tile, tile, whole((heads, depth, 2 * depth))],
        out_shape=[
            jax.ShapeDtypeStruct((rows, width), F32),
            jax.ShapeDtypeStruct((rows, width), BF16),
            jax.ShapeDtypeStruct((heads, depth, 2 * depth), F32),
        ],
        scratch_shapes=[
            pltpu.VMEM((heads, depth, 2 * depth), F32),
            pltpu.VMEM((3, HALO, width), F32),
        ],
        compiler_params=pltpu.CompilerParams(
            dimension_semantics=("arbitrary",), vmem_limit_bytes=32 * 1024 * 1024
        ),
        cost_estimate=pl.CostEstimate(
            flops=rows * width * 4096, bytes_accessed=rows * width * 12, transcendentals=0
        ),
    )(q, k, v, hq, hk, hv, taps, beta, decay)


def finish_kernel(heads, depth, out_ref, eff_ref, state_ref, gain_ref, mixed_ref):
    gain = gain_ref[...].astype(F32)
    for h in range(heads):
        cols = slice(h * depth, (h + 1) * depth)
        raw = out_ref[:, cols] + dot(eff_ref[:, cols], state_ref[h])
        scale = lax.rsqrt(jnp.mean(raw * raw, axis=-1, keepdims=True) + EPSILON)
        mixed_ref[:, cols] = (raw * scale * gain).astype(BF16)


def finish_pass(out, eff, incoming, gain):
    rows, width = out.shape
    heads, depth = incoming.shape[:2]
    chunk = min(256, rows)
    tile = pl.BlockSpec((chunk, width), lambda i: (i, 0))
    return pl.pallas_call(
        lambda *refs: finish_kernel(heads, depth, *refs),
        grid=(rows // chunk,),
        in_specs=[
            tile,
            tile,
            pl.BlockSpec(incoming.shape, lambda i: (0, 0, 0)),
            pl.BlockSpec((1, depth), lambda i: (0, 0)),
        ],
        out_specs=tile,
        out_shape=jax.ShapeDtypeStruct((rows, width), BF16),
        compiler_params=pltpu.CompilerParams(dimension_semantics=("arbitrary",)),
    )(out, eff, incoming, gain.reshape(1, depth))


def earlier_state(state, depth):
    def compose(later, earlier):
        pushed = jnp.einsum(
            "hde,hef->hdf", later[..., depth:].astype(BF16), earlier, preferred_element_type=F32
        )
        own = jnp.concatenate([later[..., :depth], jnp.zeros_like(later[..., depth:])], axis=-1)
        return own + pushed

    held = shifted_2(state.astype(BF16), "sp", 1)
    count = lax.axis_size("sp")
    distance = 1
    while distance < count - 1:
        sent = held if 2 * distance < count - 1 else held[..., :depth]
        arrived = shifted_2(sent, "sp", distance)
        if 2 * distance < count - 1:
            held = compose(held.astype(F32), arrived).astype(BF16)
        else:
            held = held[..., :depth].astype(F32) + jnp.einsum(
                "hde,hef->hdf", held[..., depth:], arrived, preferred_element_type=F32
            )
        distance *= 2
    return held[..., :depth].astype(BF16)


def per_device(
    tokens,
    input_norm_scale,
    mean_input_weight,
    query_matrix,
    key_matrix,
    value_matrix,
    strength_weight,
    decay_input_weight,
    causal_filter_weight,
    head_decay_logrates,
    decay_input_shift,
    strength_shift,
    decay_spike,
    head_norm_scale,
    group_mixing_weight,
    mean_channel_scale,
    mean_output_weight,
    delta_output_weight,
):
    tok_rows = tokens.shape[0]
    pool_cols = mean_input_weight.shape[1]
    delta_cols = query_matrix.shape[1]
    head_count = strength_weight.shape[1]
    head_depth = delta_cols // head_count
    groups_dev = pool_cols // GROUP_DIM
    tp_index = lax.axis_index("tp")
    sp_index = lax.axis_index("sp")
    normed = scale_rows(tokens.astype(jnp.float32), input_norm_scale).astype(jnp.bfloat16)
    narrow = lax.all_gather(
        jnp.concatenate([strength_weight, decay_input_weight], axis=1), "sp", axis=0, tiled=True
    )
    project = lambda weight: jnp.dot(normed, weight, preferred_element_type=F32).astype(BF16)
    gather = lambda weight: lax.all_gather(weight, "sp", axis=0, tiled=True)
    key_raw = project(gather(key_matrix))
    query_raw = project(gather(query_matrix))
    value_raw = project(gather(value_matrix))
    pool_raw = project(gather(mean_input_weight))
    narrow_raw = project(narrow)
    beta_raw = narrow_raw[:, :head_count]
    decay_unshaped = narrow_raw[:, head_count:]
    pool_reach = 15
    halos = shifted_2(
        tuple(raw[tok_rows - HALO :] for raw in (query_raw, key_raw, value_raw)), "sp", 1
    )
    previous_pool = shifted_2(pool_raw[tok_rows - pool_reach :], "sp", 1)
    taps = lax.dynamic_slice_in_dim(causal_filter_weight, tp_index * delta_cols, delta_cols, 2)
    rate_logarithm = lax.dynamic_slice_in_dim(
        head_decay_logrates, tp_index * head_count, head_count
    )
    shift_amounts = lax.dynamic_slice_in_dim(decay_input_shift, tp_index * head_count, head_count)
    strength_offsets = lax.dynamic_slice_in_dim(strength_shift, tp_index * head_count, head_count)
    beta = jax.nn.sigmoid(beta_raw.astype(jnp.float32) + strength_offsets)
    decay_logarithm = (
        -jnp.exp(rate_logarithm)
        * jax.nn.softplus(decay_unshaped.astype(jnp.float32) + shift_amounts)
        + decay_spike
    )
    out_local, out_reach, state = delta_pass(
        query_raw, key_raw, value_raw, *halos, taps, beta, decay_logarithm, head_depth
    )
    incoming = earlier_state(state, head_depth)
    delta_mixed = finish_pass(out_local, out_reach, incoming, head_norm_scale)
    group_ids = tp_index * groups_dev + jnp.arange(pool_cols) // GROUP_DIM
    positions = sp_index * tok_rows + jnp.arange(tok_rows)
    pool_diff = pool_means(previous_pool, pool_raw, group_ids, positions)
    local_mix = lax.dynamic_slice_in_dim(group_mixing_weight, tp_index * groups_dev, groups_dev, 0)
    pooled = jnp.einsum(
        "tgc,gcd->tgd",
        pool_diff.reshape(tok_rows, groups_dev, GROUP_DIM),
        local_mix,
        preferred_element_type=jnp.float32,
    )
    pool_scale = lax.dynamic_slice_in_dim(mean_channel_scale, tp_index * pool_cols, pool_cols)
    pool_mixed = (pooled.reshape(tok_rows, pool_cols) * pool_scale.astype(jnp.float32)).astype(
        jnp.bfloat16
    )
    mixed = jnp.concatenate([pool_mixed, delta_mixed], axis=1)
    pool_weight_rows, delta_weight_rows = (
        lax.all_gather(mean_output_weight, "sp", axis=1, tiled=True),
        lax.all_gather(delta_output_weight, "sp", axis=1, tiled=True),
    )
    out_weight = jnp.concatenate([pool_weight_rows, delta_weight_rows], axis=0)
    return lax.psum_scatter(
        jnp.dot(mixed, out_weight, preferred_element_type=jnp.float32).astype(jnp.bfloat16),
        "tp",
        scatter_dimension=0,
        tiled=True,
    )


def solution(mesh):
    return jax.shard_map(
        per_device,
        mesh=mesh,
        in_specs=(
            P("sp", None),
            P(),
            P("sp", "tp"),
            P("sp", "tp"),
            P("sp", "tp"),
            P("sp", "tp"),
            P("sp", "tp"),
            P("sp", "tp"),
            P(),
            P(),
            P(),
            P(),
            P("sp", "tp"),
            P(),
            P(),
            P(),
            P("tp", "sp"),
            P("tp", "sp"),
        ),
        out_specs=P(("sp", "tp"), None),
        check_vma=False,
    )
```

profile of v0, /device:TPU:20, one launch (start us, length us, event | category | flops | bytes accessed | tf_op | source)
XLA Modules:
  0.0 561.6 jit_solution(11996877387421783596)
XLA Ops:
  10.8 5.1 fusion
  16.2 26.7 %all_gather.25 = bf16[4096,8]{0,1:T(8,128)(2,1)S(1)} all-gather(bf16[512,8]{0,1:T(8,128)(2,1)S(1)} %pad_maximum_fusion), channel_id=1, replica_groups=mesh['sp'=8,'tp'=4] {'sp'}, dimensions={0}, use_global_device_ids=true | all-gather | bytes 73728 | tf_op jit(solution)/shard_map/all_gather | solution.py:272
  44.5 10.7 %fusion.2 = bf16[1024,4096]{1,0:T(8,128)(2,1)} fusion(bf16[1024,4096]{1,0:T(8,128)(2,1)} %param.18, f32[4096]{0:T(1024)S(1)} %convert_element_type.72, f32[1024]{0:T(1024)S(1)} %add_rsqrt_fusion), kind=kLoop, calls=%fused_computation.4 | loop fusion | flops 16777216 | bytes 16797696 | tf_op jit(solution)/shard_map/convert_element_type | solution.py:271
  55.3 5.7 %convolution_convert_fusion.4 = bf16[1024,8]{1,0:T(8,128)(2,1)S(1)} fusion(bf16[1024,4096]{1,0:T(8,128)(2,1)} %fusion.2, bf16[4096,8]{0,1:T(8,128)(2,1)S(1)} %all_gather.25), kind=kOutput, calls=%fused_computation.53 | convolution fusion | flops 67117056 | bytes 8470528 | tf_op jit(solution)/shard_map/dot_general | solution.py:275
  61.5 21.7 %all-gather.9.cloned.1.call-done = bf16[4096,512]{1,0:T(8,128)(2,1)} async-done(((bf16[512,512]{1,0:T(8,128)(2,1)}), bf16[4096,512]{1,0:T(8,128)(2,1)}) %all-gather.9.cloned.1.call-update) | async-done | bytes 4194320 | tf_op jit(solution)/shard_map/all_gather | solution.py:276
  83.2 9.1 %convolution_convert_fusion.2.refs_0_ = bf16[1024,512]{1,0:T(8,128)(2,1)S(1)} fusion(bf16[1024,4096]{1,0:T(8,128)(2,1)} %fusion.2, bf16[4096,512]{1,0:T(8,128)(2,1)} %all-gather.9.cloned.1.call-done), kind=kOutput, calls=%fused_computation.50 | convolution fusion | flops 4295491584 | bytes 13631488 | tf_op jit(solution)/shard_map/dot_general | solution.py:275
  95.0 61.9 %all-gather.11.cloned.1.call-done = bf16[4096,512]{1,0:T(8,128)(2,1)} async-done(((bf16[512,512]{1,0:T(8,128)(2,1)}), bf16[4096,512]{1,0:T(8,128)(2,1)}) %all-gather.11.cloned.1.call-update) | async-done | bytes 4194320 | tf_op jit(solution)/shard_map/all_gather | solution.py:276
  156.9 9.0 %convolution_convert_fusion.1.refs_1_ = bf16[1024,512]{1,0:T(8,128)(2,1)S(1)} fusion(bf16[1024,4096]{1,0:T(8,128)(2,1)} %fusion.2, bf16[4096,512]{1,0:T(8,128)(2,1)} %all-gather.11.cloned.1.call-done), kind=kOutput, calls=%fused_computation.49 | convolution fusion | flops 4295491584 | bytes 13631488 | tf_op jit(solution)/shard_map/dot_general | solution.py:275
  169.4 61.1 %all-gather.13.cloned.1.call-done = bf16[4096,512]{1,0:T(8,128)(2,1)} async-done(((bf16[512,512]{1,0:T(8,128)(2,1)}), bf16[4096,512]{1,0:T(8,128)(2,1)}) %all-gather.13.cloned.1.call-update) | async-done | bytes 4194320 | tf_op jit(solution)/shard_map/all_gather | solution.py:276
  230.6 9.1 %convolution_convert_fusion.refs_2_ = bf16[1024,512]{1,0:T(8,128)(2,1)S(1)} fusion(bf16[1024,4096]{1,0:T(8,128)(2,1)} %fusion.2, bf16[4096,512]{1,0:T(8,128)(2,1)} %all-gather.13.cloned.1.call-done), kind=kOutput, calls=%fused_computation.48 | convolution fusion | flops 4295491584 | bytes 13631488 | tf_op jit(solution)/shard_map/dot_general | solution.py:275
  242.2 4.5 collective-permute-done.3.refs_5_
  246.7 24.2 %shard_map.172 = (f32[1024,512]{1,0:T(8,128)S(1)}, bf16[1024,512]{1,0:T(8,128)(2,1)S(1)}, f32[4,128,256]{2,1,0:T(8,128)S(1)}) custom-call(bf16[1024,512]{1,0:T(8,128)(2,1)S(1)} %convolution_convert_fusion.2.refs_0_, bf16[1024,512]{1,0:T(8,128)(2,1)S(1)} %copy-done.5, bf16[1024,512]{1,0:T(8,128)(2,1)S(1)} %convolution_convert_fusion.refs_2_, ...), custom_call_target="tpu_custom_call" | custom-call | flops 2147483648 | bytes 6291456 | tf_op jit(solution)/shard_map/pallas_call | solution.py:167
  275.2 34.6 %all-gather.7.cloned.1.call-done = bf16[4096,512]{1,0:T(8,128)(2,1)} async-done(((bf16[512,512]{1,0:T(8,128)(2,1)}), bf16[4096,512]{1,0:T(8,128)(2,1)}) %all-gather.7.cloned.1.call-update) | async-done | bytes 4194320 | tf_op jit(solution)/shard_map/all_gather | solution.py:276
  309.8 9.1 %convolution_convert_fusion.3 = bf16[1024,512]{1,0:T(8,128)(2,1)S(1)} fusion(bf16[1024,4096]{1,0:T(8,128)(2,1)} %fusion.2, bf16[4096,512]{1,0:T(8,128)(2,1)} %all-gather.7.cloned.1.call-done), kind=kOutput, calls=%fused_computation.51 | convolution fusion | flops 4295491584 | bytes 13631488 | tf_op jit(solution)/shard_map/dot_general | solution.py:275
  321.4 3.2 collective-permute-start.5
  326.4 13.0 %collective-permute-done.5 = bf16[4,128,256]{2,1,0:T(8,128)(2,1)S(1)} collective-permute-done((bf16[4,128,256]{2,1,0:T(8,128)(2,1)S(1)}, bf16[4,128,256]{2,1,0:T(8,128)(2,1)S(1)}, u32[]{:S(2)}, u32[]{:S(2)}) %collective-permute-start.5) | collective-permute-done | bytes 262176 | tf_op jit(solution)/shard_map/ppermute | solution.py:20
  339.6 4.1 collective-permute-start.6
  343.6 8.2 %fusion.32 = f32[4,128,1024]{2,1,0:T(8,128)} fusion(bf16[16,128,128]{2,1,0:T(8,128)(2,1)S(1)} %copy-done, s32[]{:T(128)S(6)} %select_n.179, s32[512]{0:T(512)S(1)} %fusion.50, s32[1024]{0:T(1024)S(1)} %add_add_fusion, f32[1039,512]{1,0:T(8,128)S(1)} %maximum_convert_fusion, pred[512]{0:T(512)(128)(4,1)S(1)} %get-tuple-element.13, ...), kind=kOutput, calls=%fused_computation.56 | convolution fusion | flops 153092096 | bytes 35796996 | tf_op jit(solution)/shard_map/tgc,gcd->tgd/dot_general | solution.py:310
  356.7 8.7 %collective-permute-done.7 = bf16[4,128,128]{2,1,0:T(8,128)(2,1)S(1)} collective-permute-done((bf16[4,128,128]{2,1,0:T(8,128)(2,1)S(1)}, bf16[4,128,128]{2,1,0:T(8,128)(2,1)S(1)}, u32[]{:S(2)}, u32[]{:S(2)}) %collective-permute-start.7) | collective-permute-done | bytes 131104 | tf_op jit(solution)/shard_map/ppermute | solution.py:20
  366.2 4.6 shard_map.173
  370.7 24.9 %all-gather.15.cloned.1.call-done = bf16[512,4096]{1,0:T(8,128)(2,1)} async-done(((bf16[512,512]{1,0:T(8,128)(2,1)}), bf16[512,4096]{1,0:T(8,128)(2,1)}) %all-gather.15.cloned.1.call-update) | async-done | bytes 4194320 | tf_op jit(solution)/shard_map/all_gather | solution.py:322
  395.7 75.7 %all-gather.17.cloned.1.call-done = bf16[512,4096]{1,0:T(8,128)(2,1)} async-done(((bf16[512,512]{1,0:T(8,128)(2,1)}), bf16[512,4096]{1,0:T(8,128)(2,1)}) %all-gather.17.cloned.1.call-update) | async-done | bytes 4194320 | tf_op jit(solution)/shard_map/all_gather | solution.py:323
  471.4 13.6 %fusion.7 = bf16[1024,4096]{1,0:T(8,128)(2,1)} fusion(bf16[512,4096]{1,0:T(8,128)(2,1)} %all-gather.17.cloned.1.call-done, bf16[512,4096]{1,0:T(8,128)(2,1)} %all-gather.15.cloned.1.call-done, bf16[1024,512]{1,0:T(8,128)(2,1)} %shard_map.173, bf16[1024,512]{1,0:T(8,128)(2,1)S(1)} %copy-done.6), kind=kOutput, calls=%fused_computation.9 | convolution fusion | flops 8615100416 | bytes 18874368 | tf_op jit(solution)/shard_map/dot_general | solution.py:327
  485.0 69.7 %reduce-scatter.2.cloned.1.call-done = bf16[256,4096]{1,0:T(8,128)(2,1)} async-done(((bf16[1024,4096]{1,0:T(8,128)(2,1)}), bf16[256,4096]{1,0:T(8,128)(2,1)}) %reduce-scatter.2.cloned.1.call-update) | async-done | bytes 2097168 | tf_op jit(solution)/shard_map/reduce_scatter | solution.py:326
  (88 shorter events, 29.5 us)
Async XLA Ops:
  6.5 337.1 %copy-start = (bf16[16,128,128]{2,1,0:T(8,128)(2,1)S(1)}, bf16[16,128,128]{2,1,0:T(8,128)(2,1)}, u32[]{:S(2)}) copy-start(bf16[16,128,128]{2,1,0:T(8,128)(2,1)} %param.32) | copy-start | bytes 1572868
  6.5 76.7 %all-gather.9.cloned.1.call-start = ((), (), s32[]{:S(2)}) async-start(), calls=%async_computation.2 | async-start | bytes 4718592 | tf_op jit(solution)/shard_map/all_gather | solution.py:276
  7.3 149.6 %all-gather.11.cloned.1.call-start = ((), (), s32[]{:S(2)}) async-start(), calls=%async_computation.3 | async-start | bytes 4718592 | tf_op jit(solution)/shard_map/all_gather | solution.py:276
  8.0 222.5 %all-gather.13.cloned.1.call-start = ((), (), s32[]{:S(2)}) async-start(), calls=%async_computation.4 | async-start | bytes 4718592 | tf_op jit(solution)/shard_map/all_gather | solution.py:276
  8.7 301.0 %all-gather.7.cloned.1.call-start = ((), (), s32[]{:S(2)}) async-start(), calls=%async_computation.1 | async-start | bytes 4718592 | tf_op jit(solution)/shard_map/all_gather | solution.py:276
  9.3 386.4 %all-gather.15.cloned.1.call-start = ((), (), s32[]{:S(2)}) async-start(), calls=%async_computation.5 | async-start | bytes 4718592 | tf_op jit(solution)/shard_map/all_gather | solution.py:322
  9.9 461.5 %all-gather.17.cloned.1.call-start = ((), (), s32[]{:S(2)}) async-start(), calls=%async_computation.6 | async-start | bytes 4718592 | tf_op jit(solution)/shard_map/all_gather | solution.py:323
  10.5 544.3 %reduce-scatter.2.cloned.1.call-start = ((), (), s32[]{:S(2)}) async-start(), calls=%async_computation.7 | async-start | bytes 10485760 | tf_op jit(solution)/shard_map/reduce_scatter | solution.py:326
  10.7 5.3 copy-start.13
  10.7 5.4 copy-start.9
  10.7 5.4 copy-start.10
  10.7 32.1 %copy-start.7 = (f32[1024,4]{0,1:T(4,128)S(1)}, f32[1024,4]{0,1:T(4,128)}, u32[]{:S(2)}) copy-start(f32[1024,4]{0,1:T(4,128)} %param.30) | copy-start | bytes 49156
  92.3 150.0 %collective-permute-start.1 = (bf16[8,512]{1,0:T(8,128)(2,1)S(1)}, bf16[8,512]{1,0:T(8,128)(2,1)S(1)}, u32[]{:S(2)}, u32[]{:S(2)}) collective-permute-start(bf16[8,512]{1,0:T(8,128)(2,1)S(1)} %slice.129), channel_id=1, source_target_pairs={{0,4},{4,8},{8,12},{12,16},{16,20},{20,24},{24,28},{1,5},{5,9},{9,... | collective-permute-start | bytes 24584 | tf_op jit(solution)/shard_map/ppermute | solution.py:20
  166.9 75.3 %collective-permute-start.2 = (bf16[8,512]{1,0:T(8,128)(2,1)S(1)}, bf16[8,512]{1,0:T(8,128)(2,1)S(1)}, u32[]{:S(2)}, u32[]{:S(2)}) collective-permute-start(bf16[8,512]{1,0:T(8,128)(2,1)S(1)} %slice.130), channel_id=1, source_target_pairs={{0,4},{4,8},{8,12},{12,16},{16,20},{20,24},{24,28},{1,5},{5,9},{9,... | collective-permute-start | bytes 24584 | tf_op jit(solution)/shard_map/ppermute | solution.py:20
  230.6 16.2 %copy-start.5 = (bf16[1024,512]{1,0:T(8,128)(2,1)S(1)}, bf16[1024,512]{1,0:T(8,128)(2,1)}, u32[]{:S(2)}) copy-start(bf16[1024,512]{1,0:T(8,128)(2,1)} %copy-done.4) | copy-start | bytes 3145732
  239.7 7.0 %collective-permute-start.3 = (bf16[8,512]{1,0:T(8,128)(2,1)S(1)}, bf16[8,512]{1,0:T(8,128)(2,1)S(1)}, u32[]{:S(2)}, u32[]{:S(2)}) collective-permute-start(bf16[8,512]{1,0:T(8,128)(2,1)S(1)} %slice.131), channel_id=1, source_target_pairs={{0,4},{4,8},{8,12},{12,16},{16,20},{20,24},{24,28},{1,5},{5,9},{9,... | collective-permute-start | bytes 24584 | tf_op jit(solution)/shard_map/ppermute | solution.py:20
  273.2 48.1 %collective-permute-start.4 = (bf16[4,128,256]{2,1,0:T(8,128)(2,1)S(1)}, bf16[4,128,256]{2,1,0:T(8,128)(2,1)S(1)}, u32[]{:S(2)}, u32[]{:S(2)}) collective-permute-start(bf16[4,128,256]{2,1,0:T(8,128)(2,1)S(1)} %convert_element_type.86), channel_id=1, source_target_pairs={{0,4},{4,8},{8,12},{12,16},{16,20},{20,24},{24,28},{1,5},{5,9},{9,... | collective-permute-start | bytes 786440 | tf_op jit(solution)/shard_map/ppermute | solution.py:20
  318.8 20.5 %copy-start.14 = (pred[256]{0:T(512)(128)(4,1)S(1)}, pred[256]{0:T(512)(128)(4,1)}, u32[]{:S(2)}) copy-start(pred[256]{0:T(512)(128)(4,1)} %constant.125.clone.1) | copy-start | bytes 772
  318.9 7.2 %collective-permute-start = (bf16[15,512]{1,0:T(8,128)(2,1)S(1)}, bf16[15,512]{1,0:T(8,128)(2,1)S(1)}, u32[]{:S(2)}, u32[]{:S(2)}) collective-permute-start(bf16[15,512]{1,0:T(8,128)(2,1)S(1)} %slice.112), channel_id=1, source_target_pairs={{0,4},{4,8},{8,12},{12,16},{16,20},{20,24},{24,28},{1,5},{5,9},{9,... | collective-permute-start | bytes 46088 | tf_op jit(solution)/shard_map/ppermute | solution.py:20
  321.4 18.0 %collective-permute-start.5 = (bf16[4,128,256]{2,1,0:T(8,128)(2,1)S(1)}, bf16[4,128,256]{2,1,0:T(8,128)(2,1)S(1)}, u32[]{:S(2)}, u32[]{:S(2)}) collective-permute-start(bf16[4,128,256]{2,1,0:T(8,128)(2,1)S(1)} %collective-permute-done.4), channel_id=1, source_target_pairs={{0,4},{4,8},{8,12},{12,16},{16,20},{20,24},{24,28},{1,5},{5,9},{9,... | collective-permute-start | bytes 786440 | tf_op jit(solution)/shard_map/ppermute | solution.py:20
  339.6 14.3 %collective-permute-start.6 = (bf16[4,128,256]{2,1,0:T(8,128)(2,1)S(1)}, bf16[4,128,256]{2,1,0:T(8,128)(2,1)S(1)}, u32[]{:S(2)}, u32[]{:S(2)}) collective-permute-start(bf16[4,128,256]{2,1,0:T(8,128)(2,1)S(1)} %fusion.31), channel_id=1, source_target_pairs={{0,8},{4,12},{8,16},{12,20},{16,24},{20,28},{1,9},{5,13},{9,17},{1... | collective-permute-start | bytes 786440 | tf_op jit(solution)/shard_map/ppermute | solution.py:20
  354.1 11.3 %collective-permute-start.7 = (bf16[4,128,128]{2,1,0:T(8,128)(2,1)S(1)}, bf16[4,128,128]{2,1,0:T(8,128)(2,1)S(1)}, u32[]{:S(2)}, u32[]{:S(2)}) collective-permute-start(bf16[4,128,128]{2,1,0:T(8,128)(2,1)S(1)} %slice.136), channel_id=1, source_target_pairs={{0,16},{4,20},{8,24},{12,28},{1,17},{5,21},{9,25},{13,29},{2,18},{... | collective-permute-start | bytes 393224 | tf_op jit(solution)/shard_map/ppermute | solution.py:20
  366.2 105.2 %copy-start.6 = (bf16[1024,512]{1,0:T(8,128)(2,1)S(1)}, bf16[1024,512]{1,0:T(8,128)(2,1)}, u32[]{:S(2)}) copy-start(bf16[1024,512]{1,0:T(8,128)(2,1)} %multiply_convert_fusion) | copy-start | bytes 3145732
  485.0 69.7 %copy-start.1 = (bf16[16,128,128]{2,1,0:T(8,128)(2,1)S(1)}, bf16[16,128,128]{2,1,0:T(8,128)(2,1)}, u32[]{:S(2)}) copy-start(bf16[16,128,128]{2,1,0:T(8,128)(2,1)} %param.32) | copy-start | bytes 1572868
  (6 other events, 17.9 us)
Sparse Core Ops, SparseCore 0:
  9.5 73.6 all-gather.8
  85.3 71.5 all-gather.10
  159.0 71.4 all-gather.12
  232.5 77.1 all-gather.6
  311.7 83.9 all-gather.14
  397.6 73.7 all-gather.16
  485.2 69.5 reduce-scatter.1
where the time goes:
time: 565 us; the launch traced here: 562 us
  waiting for transfers between devices  381 us (67%)
  matrix products  65.1 us (12%)
  Pallas kernels  28.7 us (5%)
  blocking collectives  26.7 us (5%)
  starting transfers between devices  20.8 us (4%)
  other arithmetic  19 us (3%)
  between operations  13.9 us (2%)
  local copies, waits for them, and re-layouts  6.47 us (1%)
    all_gather x4, waiting for transfers between devices, per_device(): gather = lambda weight: lax.all_gather(weight, 'sp', axis=0, tiled=True)  179 us
    all_gather x1, waiting for transfers between devices, per_device(): lax.all_gather(delta_output_weight, 'sp', axis=1, tiled=True)  75.7 us
    reduce_scatter x1, waiting for transfers between devices, per_device(): lax.psum_scatter(jnp.dot(mixed, out_weight, preferred_element_type=jnp.fl...  69.7 us
    dot_general x5, matrix products, per_device(): jnp.dot(normed, weight, preferred_element_type=F32).astype(BF16)  42 us
    ppermute x8, waiting for transfers between devices, shifted_2(): return lax.ppermute(block, axis, route)  27.6 us
    all_gather x1, blocking collectives, per_device(): lax.all_gather(jnp.concatenate([strength_weight, decay_input_weight], axi...  26.7 us
    all_gather x1, waiting for transfers between devices, per_device(): lax.all_gather(mean_output_weight, 'sp', axis=1, tiled=True)  24.9 us
    pallas_call x1, Pallas kernels, delta_pass(): pl.pallas_call(lambda *refs: delta_kernel(heads, depth, chunk, *refs), gr...  24.2 us
  transfers between devices with their start and end apart: 15, of which 11 were waited for; matrix products, arithmetic and copies ran while one was open for 13% of the time, Pallas kernels for 5%

commit v1 on v0

v1 whole, which is shorter than its diff:
```python
import jax
import jax.numpy as jnp
from jax import lax
from jax.experimental import pallas as pl
from jax.experimental.pallas import tpu as pltpu
from jax.sharding import PartitionSpec as P

GROUP_DIM = 128
CONV = 4
EPSILON = 1e-06
PAD = 16
CHUNK = 128
BF16 = jnp.bfloat16
F32 = jnp.float32
MESH = pl.DeviceIdType.MESH
KEY, VAL, QRY, POOL = range(4)


def dot(left, right):
    return jnp.dot(left.astype(BF16), right.astype(BF16), preferred_element_type=F32)


def dot_nt(left, right):
    return lax.dot_general(
        left.astype(BF16),
        right.astype(BF16),
        (((1,), (1,)), ((), ())),
        preferred_element_type=F32,
    )


def dot_tn(left, right):
    return lax.dot_general(
        left.astype(BF16),
        right.astype(BF16),
        (((0,), (0,)), ((), ())),
        preferred_element_type=F32,
    )


def unit_rows(values):
    return values * lax.rsqrt(jnp.sum(values * values, axis=-1, keepdims=True) + EPSILON)


def delta_chunk(heads, depth, chunk, qkv, taps, beta, decay, carry):
    width = heads * depth
    row = lax.broadcasted_iota(jnp.int32, (chunk, chunk), 0)
    col = lax.broadcasted_iota(jnp.int32, (chunk, chunk), 1)
    causal = row >= col
    strict = row > col
    eye = jnp.where(row == col, 1.0, 0.0)
    convolved = []
    for r in range(3):
        extended = qkv[r].astype(F32)
        total = jnp.zeros((chunk, width), F32)
        for i in range(CONV):
            start = PAD - (CONV - 1) + i
            total = total + taps[i][r] * extended[start : start + chunk]
        convolved.append(total / (1.0 + jnp.exp(-total)))
    tri = jnp.where(causal, 1.0, 0.0)
    cum_cols = jnp.dot(tri, decay, preferred_element_type=F32, precision=lax.Precision.HIGHEST)
    cum_rows = lax.dot_general(
        decay,
        tri,
        (((0,), (1,)), ((), ())),
        preferred_element_type=F32,
        precision=lax.Precision.HIGHEST,
    )
    base = min(16, chunk)
    hs = range(heads)
    q = [unit_rows(convolved[0][:, h * depth : (h + 1) * depth]) * depth ** (-0.5) for h in hs]
    k = [unit_rows(convolved[1][:, h * depth : (h + 1) * depth]) for h in hs]
    v = [convolved[2][:, h * depth : (h + 1) * depth] for h in hs]
    cum = [cum_cols[:, h : h + 1] for h in hs]
    last = [cum_cols[chunk - 1 : chunk, h : h + 1] for h in hs]
    beta = [beta[:, h : h + 1] for h in hs]
    weights = [
        jnp.where(causal, jnp.exp(jnp.where(causal, cum[h] - cum_rows[h : h + 1, :], 0.0)), 0.0)
        for h in hs
    ]
    kb = [k[h] * beta[h] for h in hs]
    lower = [jnp.where(strict, dot_nt(kb[h], k[h]) * weights[h], 0.0) for h in hs]
    power = [jnp.where(row // base == col // base, lower[h], 0.0) for h in hs]
    inverse = [eye - power[h] for h in hs]
    reach = 2
    while reach < base:
        power = [dot(power[h], power[h]) for h in hs]
        inverse = [inverse[h] + dot(inverse[h], power[h]) for h in hs]
        reach *= 2
    size = base
    while size < chunk:
        pair = (row // (2 * size) == col // (2 * size)) & (row // size != col // size)
        right = [dot(jnp.where(pair, lower[h], 0.0), inverse[h]) for h in hs]
        inverse = [inverse[h] - dot(inverse[h], right[h]) for h in hs]
        size *= 2
    grow = [jnp.exp(cum[h]) for h in hs]
    sides = [jnp.concatenate([v[h] * beta[h], kb[h] * grow[h]], axis=1) for h in hs]
    solved = [dot(inverse[h], sides[h]) for h in hs]
    scores = [dot_nt(q[h], k[h]) * weights[h] for h in hs]
    kd = [k[h] * jnp.exp(last[h] - cum[h]) for h in hs]
    zeros = jnp.zeros((chunk, depth), F32)
    state = [carry[h] for h in hs]
    fresh = [
        jnp.concatenate([solved[h][:, :depth], zeros], axis=1) - dot(solved[h][:, depth:], state[h])
        for h in hs
    ]
    outs = [dot(q[h] * grow[h], state[h]) + dot(scores[h], fresh[h]) for h in hs]
    for h in hs:
        carry[h] = state[h] * jnp.exp(last[h]) + dot_tn(kd[h], fresh[h])
    return outs


class Ring:
    def __init__(self, hops, half_rows, refs, sems, owner, peers, window):
        self.refs, self.sems, self.owner, self.peers, self.window = refs, sems, owner, peers, window
        self.items = []
        self.index = {}
        rows_in, rows_out = half_rows
        for j in range(1, hops + 1):
            for m in (KEY, VAL, QRY):
                top = rows_in // 2
                full = rows_in + PAD if m == KEY else rows_in
                if j < hops:
                    self.add(("in", m, 0), j, [("in", m, 0, full)] * 2)
                else:
                    self.add(("in", m, 0), j, [("in", m, 0, top), ("in", m, top, full)])
        top = rows_in // 2
        for j in range(1, hops + 1):
            if j < hops:
                self.add(("in", POOL, 0), j, [("in", POOL, 0, top)] * 2)
                self.add(("in", POOL, 1), j, [("in", POOL, top, rows_in)] * 2)
            else:
                self.add(("in", POOL, 0), j, [("in", POOL, 0, top), ("in", POOL, top, rows_in)])
        for j in range(1, hops + 1):
            if j < hops:
                self.add(("out", 0, 0), j, [("out", 0, 0, rows_out)] * 2)
                self.add(("out", 1, 0), j, [("out", 1, 0, rows_out)] * 2)
            else:
                self.add(("out", 0, 0), j, [("out", 0, 0, rows_out), ("out", 1, 0, rows_out)])
        self.finish = []
        total = 0
        for _, _, parts in self.items:
            total += parts[0][3] - parts[0][2]
            self.finish.append(total)
        self.total = total
        self.started = 0
        self.sent = set()
        self.received = set()

    def add(self, key, j, parts):
        self.index[key + (j,)] = len(self.items)
        self.items.append((key, j, parts))

    def copy(self, i, side):
        key, j, parts = self.items[i]
        kind, m, low, high = parts[side]
        ref = self.refs[kind]
        block = ref.at[m, self.owner(-(j - 1) if side == 0 else j - 1), pl.ds(low, high - low), :]
        return pltpu.make_async_remote_copy(
            src_ref=block,
            dst_ref=block,
            send_sem=self.sems[0].at[i, side],
            recv_sem=self.sems[1].at[i, side],
            device_id=self.peers[side],
            device_id_type=MESH,
        )

    def arrive(self, i, side):
        if (i, side) in self.received:
            return
        self.received.add((i, side))
        self.copy(i, side).wait_recv()

    def leave(self, i):
        if i in self.sent:
            return
        self.sent.add(i)
        for side in range(2):
            self.copy(i, side).wait_send()

    def start_next(self):
        i = self.started
        if i >= len(self.items):
            return
        if i >= self.window:
            self.leave(i - self.window)
        key, j, parts = self.items[i]
        for side in range(2):
            if j > 1:
                kind, m, low, high = parts[side]
                for before in range(i):
                    other, hop, pieces = self.items[before]
                    if hop == j - 1 and pieces[side][:2] == (kind, m) and pieces[side][2] <= low < pieces[side][3]:
                        self.arrive(before, side)
                    elif hop == j - 1 and pieces[side][:2] == (kind, m) and low <= pieces[side][2] < high:
                        self.arrive(before, side)
            self.copy(i, side).start()
        self.started += 1

    def tick(self, part):
        while self.started < len(self.items):
            behind = self.started - self.window
            if behind >= 0 and self.finish[behind] > part * self.total:
                break
            self.start_next()

    def need(self, key):
        i = self.index[key]
        while self.started < min(len(self.items), i + self.window + 1):
            self.start_next()
        for side in range(2):
            self.arrive(i, side)

    def close(self):
        while self.started < len(self.items):
            self.start_next()
        for i in range(len(self.items)):
            for side in range(2):
                self.arrive(i, side)
            self.leave(i)


def mixer_kernel(cfg, *refs):
    (
        tok_ref, gain_ref, wk_ref, wv_ref, wq_ref, wp_ref, narrow_ref, tap_ref, rate_ref, dshift_ref,
        sshift_ref, spike_ref, hgain_ref, gmw_ref, cscale_ref, wpo_ref, wdo_ref,
    ) = refs[:17]
    out_ref = refs[17]
    (
        win, wout, normed, acc, raw, stage, nraw, gmw, carry, held, caught, psend, corerecv, ysend, yrecv,
        obuf, ring_send, ring_recv, local_sem, tok_sem, halo_send, halo_recv, scan_send, scan_recv,
        core_send, core_recv, y_send, y_recv, out_sem,
    ) = refs[18:]
    n_sp, n_tp, heads, depth, grid_x = cfg
    grid_z = n_sp // grid_x
    hops = n_sp // 2
    n_y = n_tp // 2
    rows, width = raw.shape[1] - PAD, raw.shape[2]
    rows_in = normed.shape[2]
    cols_out = wout.shape[3]
    share = rows // n_tp
    sp = lax.axis_index("sp")
    tp = lax.axis_index("tp")
    core = tp % 2
    ypos = tp // 2

    def sp_at(r):
        s = jnp.maximum(r - grid_z, 0)
        i = s // (grid_x - 1)
        k = s % (grid_x - 1)
        x = 1 + jnp.where(i % 2 == 0, k, grid_x - 2 - k)
        return jnp.where(r < grid_z, r * grid_x, (grid_z - 1 - i) * grid_x + x)

    zc = sp // grid_x
    xc = sp % grid_x
    ic = grid_z - 1 - zc
    kc = jnp.where(ic % 2 == 0, xc - 1, grid_x - 1 - xc)
    pos = jnp.where(xc == 0, zc, grid_z + ic * (grid_x - 1) + kc)

    def owner(offset):
        return sp_at((pos + offset + n_sp) % n_sp)

    locals_ = []

    def bring(src, dst):
        locals_.append(pltpu.make_async_copy(src, dst, local_sem.at[len(locals_)]))
        locals_[-1].start()

    bring(wk_ref, win.at[KEY, sp, pl.ds(0, rows_in), :])
    bring(narrow_ref, win.at[KEY, sp, pl.ds(rows_in, PAD), :])
    bring(wv_ref, win.at[VAL, sp, pl.ds(0, rows_in), :])
    bring(wq_ref, win.at[QRY, sp, pl.ds(0, rows_in), :])
    bring(wp_ref, win.at[POOL, sp, pl.ds(0, rows_in), :])
    bring(wpo_ref, wout.at[0, sp])
    bring(wdo_ref, wout.at[1, sp])
    groups = gmw.shape[0]
    bring(gmw_ref.at[pl.ds(tp * groups, groups)], gmw)
    step_rows = stage.shape[1]
    n_stage = rows // step_rows

    def token_copy(t, slot):
        return pltpu.make_async_copy(
            tok_ref.at[pl.ds(pl.multiple_of(t * step_rows, step_rows), step_rows), :],
            stage.at[slot],
            tok_sem.at[slot],
        )

    token_copy(0, 0).start()

    barrier = pltpu.get_barrier_semaphore()
    for k in range(1, n_sp):
        pl.semaphore_signal(barrier, inc=1, device_id=((sp + k) % n_sp, tp), device_id_type=MESH)
    for k in range(1, n_tp):
        pl.semaphore_signal(barrier, inc=1, device_id=(sp, (tp + k) % n_tp), device_id_type=MESH)
    for c in locals_:
        c.wait()
    pl.semaphore_wait(barrier, n_sp + n_tp - 2)

    ring = Ring(
        hops,
        (rows_in, wout.shape[2]),
        {"in": win, "out": wout},
        (ring_send, ring_recv),
        owner,
        [(owner(1), tp), (owner(-1), tp)],
        2,
    )
    ring.tick(0.0)

    def norm_step(t, _):
        slot = t % 2
        token_copy(t, slot).wait()

        @pl.when(t + 1 < n_stage)
        def _():
            token_copy(t + 1, 1 - slot).start()

        def piece(u, _):
            at = pl.ds(pl.multiple_of(u * 32, 32), 32)
            squares = jnp.zeros((32, 1), F32)
            for b in range(n_sp):
                x = stage[slot, at, b * rows_in : (b + 1) * rows_in].astype(F32)
                squares = squares + jnp.sum(x * x, axis=-1, keepdims=True)
            scale = lax.rsqrt(squares * (1.0 / (n_sp * rows_in)) + EPSILON)
            to = pl.ds(pl.multiple_of(t * step_rows + u * 32, 32), 32)
            for b in range(n_sp):
                cols = slice(b * rows_in, (b + 1) * rows_in)
                x = stage[slot, at, cols].astype(F32)
                normed[b, to, :] = (x * scale * gain_ref[:, cols].astype(F32)).astype(BF16)
            return 0

        lax.fori_loop(0, step_rows // 32, piece, 0)
        return 0

    lax.fori_loop(0, n_stage, norm_step, 0)

    tile = min(256, rows)
    n_tile = rows // tile

    def project(m, owners, first=False, final=False):
        def body(t, _):
            at = pl.ds(pl.multiple_of(t * tile, tile), tile)
            total = None if first else acc[m, at, :]
            for o in owners:
                term = jnp.dot(
                    normed[o, at, :], win[m, o, pl.ds(0, rows_in), :], preferred_element_type=F32
                )
                total = term if total is None else total + term
            if final:
                raw[m, pl.ds(pl.multiple_of(PAD + t * tile, PAD), tile), :] = total.astype(BF16)
            else:
                acc[m, at, :] = total
            return 0

        lax.fori_loop(0, n_tile, body, 0)

    def halo(m):
        return pltpu.make_async_remote_copy(
            src_ref=raw.at[m, pl.ds(rows, PAD), :],
            dst_ref=raw.at[m, pl.ds(0, PAD), :],
            send_sem=halo_send.at[m],
            recv_sem=halo_recv.at[m],
            device_id=((sp + 1) % n_sp, tp),
            device_id_type=MESH,
        )

    def halo_start(m):
        @pl.when(sp + 1 < n_sp)
        def _():
            halo(m).start()

        @pl.when(sp == 0)
        def _():
            raw[m, pl.ds(0, PAD), :] = jnp.zeros((PAD, width), BF16)

    def halo_wait(m):
        @pl.when(sp > 0)
        def _():
            halo(m).wait_recv()

    def own(m, _):
        project(m, [sp], first=True)
        return 0

    lax.fori_loop(0, 4, own, 0)

    def arriving(i, _):
        for k in range(3 * hops):
            @pl.when(i == k)
            def _():
                ring.need(("in", k % 3, 0, k // 3 + 1))

        m, j = i % 3, i // 3 + 1

        @pl.when(j < hops)
        def _():
            project(m, [owner(-j), owner(j)])

        @pl.when(j == hops)
        def _():
            project(m, [owner(hops)], final=True)
            for k in range(3):
                @pl.when(m == k)
                def _():
                    halo_start(k)

        return 0

    lax.fori_loop(0, 3 * hops, arriving, 0)

    def narrow_body(t, _):
        at = pl.ds(pl.multiple_of(t * tile, tile), tile)
        total = jnp.zeros((tile, PAD), F32)
        for o in range(n_sp):
            total = total + dot_nt(normed[o, at, :], win[KEY, o, pl.ds(rows_in, PAD), :])
        nraw[at, :] = total
        return 0

    lax.fori_loop(0, n_tile, narrow_body, 0)

    lane = lax.broadcasted_iota(jnp.int32, (1, rate_ref.shape[1]), 1)
    small = lax.broadcasted_iota(jnp.int32, (1, heads), 1)

    def head_row(ref):
        total = jnp.zeros((1, heads), F32)
        for h in range(heads):
            value = jnp.sum(jnp.where(lane == tp * heads + h, ref[...], 0.0), axis=-1, keepdims=True)
            total = total + jnp.where(small == h, value, 0.0)
        return total

    speed = -jnp.exp(head_row(rate_ref))
    dshift = head_row(dshift_ref)
    sshift = head_row(sshift_ref)
    mine = pl.ds(pl.multiple_of(tp * width, 128), width)
    wide = lax.broadcasted_iota(jnp.int32, (depth, 2 * depth), 1)
    sub = lax.broadcasted_iota(jnp.int32, (depth, 2 * depth), 0)
    for h in range(heads):
        carry[h] = jnp.where(wide == sub + depth, 1.0, 0.0)
    for m in (KEY, VAL, QRY):
        halo_wait(m)
    chunk = min(CHUNK, rows)
    n_chunk = rows // chunk
    done_in = 3.0 / 6.0

    def delta_step(c, _):
        for k in range(n_chunk):
            @pl.when(c == k)
            def _():
                ring.tick(done_in + 0.03 + 0.11 * k / n_chunk)

        at = pl.ds(pl.multiple_of(c * chunk, chunk), chunk)
        window = pl.ds(pl.multiple_of(c * chunk, chunk), chunk + PAD)
        qkv = [raw[m, window, :] for m in (QRY, KEY, VAL)]
        taps = [[tap_ref[i, r : r + 1, mine].astype(F32) for r in range(3)] for i in range(CONV)]
        narrow = nraw[at, :].astype(BF16).astype(F32)
        beta = 1.0 / (1.0 + jnp.exp(-(narrow[:, :heads] + sshift)))
        x = narrow[:, heads : 2 * heads] + dshift
        soft = jnp.maximum(x, 0.0) + jnp.log1p(jnp.exp(-jnp.abs(x)))
        decay = speed * soft + spike_ref[at, :]
        outs = delta_chunk(heads, depth, chunk, qkv, taps, beta, decay, carry)
        for h in range(heads):
            cols = slice(h * depth, (h + 1) * depth)
            acc[0, at, cols] = outs[h][:, :depth]
            acc[1, at, cols] = outs[h][:, depth:]
        return 0

    lax.fori_loop(0, n_chunk, delta_step, 0)

    def halo_leave(m):
        @pl.when(sp + 1 < n_sp)
        def _():
            halo(m).wait_send()

    for m in (KEY, VAL, QRY):
        halo_leave(m)

    distances = [1]
    while 2 * distances[-1] < n_sp - 1:
        distances.append(2 * distances[-1])
    shifts = [1] + distances
    n_round = len(shifts)

    def scan_copy(r, source):
        last = r == n_round - 1
        pick = pl.ds(0, depth if last else 2 * depth)
        return pltpu.make_async_remote_copy(
            src_ref=source.at[:, :, pick],
            dst_ref=caught.at[r, :, :, pick],
            send_sem=scan_send.at[r],
            recv_sem=scan_recv.at[r],
            device_id=((sp + shifts[r]) % n_sp, tp),
            device_id_type=MESH,
        )

    def scan_start(r, source):
        @pl.when(sp + shifts[r] < n_sp)
        def _():
            scan_copy(r, source).start()

    def scan_wait(r, source):
        @pl.when(sp >= shifts[r])
        def _():
            scan_copy(r, source).wait_recv()

        @pl.when(sp < shifts[r])
        def _():
            caught[r] = jnp.zeros(caught.shape[1:], BF16)

    pool_hops = []
    for j in range(1, hops):
        pool_hops.append(j)
    for h in range(heads):
        held[0, h] = carry[h].astype(BF16)
    sources = [held.at[0]]
    scan_start(0, sources[0])

    def pool_hop(j):
        if j < hops:
            ring.need(("in", POOL, 0, j))
            ring.need(("in", POOL, 1, j))
            project(POOL, [owner(-j), owner(j)])
        else:
            ring.need(("in", POOL, 0, j))
            project(POOL, [owner(hops)], final=True)
            halo_start(POOL)

    per_round = max(1, -(-hops // max(1, n_round - 1)))
    next_hop = 1
    for r in range(n_round):
        while next_hop <= hops and next_hop <= per_round * (r + 1) and r < n_round - 1:
            pool_hop(next_hop)
            next_hop += 1
        if r == n_round - 1:
            while next_hop <= hops:
                pool_hop(next_hop)
                next_hop += 1
            ring.tick(done_in + 0.22)
            halo_wait(POOL)
            pool_mix(
                cfg, raw, gmw, cscale_ref, sp, tp, tile, rows, width,
            )
        scan_wait(r, sources[r])
        if r == 0:
            sources.append(caught.at[0])
        elif r < n_round - 1:
            before = sources[r]
            for h in range(heads):
                later = before[h]
                own_part = later[:, :depth].astype(F32)
                pushed = dot(later[:, depth:], caught[r, h])
                held[r, h, :, pl.ds(0, depth)] = (own_part + pushed[:, :depth]).astype(BF16)
                held[r, h, :, pl.ds(depth, depth)] = pushed[:, depth:].astype(BF16)
            sources.append(held.at[r])
        else:
            before = sources[r]
            for h in range(heads):
                later = before[h]
                pushed = dot(later[:, depth:], caught[r, h, :, pl.ds(0, depth)])
                held[r, h, :, pl.ds(0, depth)] = (later[:, :depth].astype(F32) + pushed).astype(BF16)
        if r + 1 < n_round:
            scan_start(r + 1, sources[r + 1])
    incoming = held.at[n_round - 1]
    ring.tick(done_in + 0.26)

    hgain = hgain_ref[...].astype(F32)

    def finish_step(t, _):
        at = pl.ds(pl.multiple_of(t * tile, tile), tile)
        to = pl.ds(pl.multiple_of(PAD + t * tile, PAD), tile)
        for h in range(heads):
            cols = slice(h * depth, (h + 1) * depth)
            value = acc[0, at, cols] + dot(acc[1, at, cols], incoming[h, :, pl.ds(0, depth)])
            scale = lax.rsqrt(jnp.mean(value * value, axis=-1, keepdims=True) + EPSILON)
            raw[VAL, to, cols] = (value * scale * hgain).astype(BF16)
        return 0

    lax.fori_loop(0, n_tile, finish_step, 0)

    def block_of(k):
        step = (k + 1) // 2
        return owner(jnp.where(k % 2 == 1, -step, step))

    def partial(dest, o):
        at = pl.ds(pl.multiple_of(PAD + dest * share, PAD), share)
        return jnp.dot(raw[KEY, at, :], wout[0, o], preferred_element_type=F32) + jnp.dot(
            raw[VAL, at, :], wout[1, o], preferred_element_type=F32
        )

    def core_copy(k):
        return pltpu.make_async_remote_copy(
            src_ref=psend.at[k % 2],
            dst_ref=corerecv.at[k],
            send_sem=core_send.at[k],
            recv_sem=core_recv.at[k],
            device_id=(sp, ypos * 2 + 1 - core),
            device_id_type=MESH,
        )

    def y_copy(k, d):
        return pltpu.make_async_remote_copy(
            src_ref=ysend.at[k, d - 1],
            dst_ref=yrecv.at[k, d - 1],
            send_sem=y_send.at[k, d - 1],
            recv_sem=y_recv.at[k, d - 1],
            device_id=(sp, ((ypos + d) % n_y) * 2 + core),
            device_id_type=MESH,
        )

    def out_copy(k):
        return pltpu.make_async_copy(
            obuf.at[k % 2],
            out_ref.at[:, pl.ds(pl.multiple_of(block_of(k) * cols_out, 128), cols_out)],
            out_sem.at[k % 2],
        )

    own_rows = acc

    def own_at(k, y):
        flat = (k % 2) * n_y + y
        return own_rows.at[2, pl.ds(pl.multiple_of(flat * share, share), share), pl.ds(0, cols_out)]

    def stage_one(k):
        o = block_of(k)

        @pl.when(k >= 2)
        def _():
            core_copy(k - 2).wait_send()

        for y in range(n_y):
            psend[k % 2, y] = partial(y * 2 + 1 - core, o).astype(BF16)
        core_copy(k).start()

    def stage_two(k):
        o = block_of(k)
        mine_now = partial(ypos * 2 + core, o).astype(BF16).astype(F32)
        parts = [partial(((ypos + d) % n_y) * 2 + core, o).astype(BF16).astype(F32) for d in range(1, n_y)]
        core_copy(k).wait_recv()
        for d in range(1, n_y):
            there = (ypos + d) % n_y
            ysend[k, d - 1] = (parts[d - 1] + corerecv[k, there].astype(F32)).astype(BF16)
            y_copy(k, d).start()
        own_at(k, 0)[...] = mine_now + corerecv[k, ypos].astype(F32)

    def stage_three(k):
        total = own_at(k, 0)[...]
        for d in range(1, n_y):
            y_copy(k, d).wait_recv()
            total = total + yrecv[k, d - 1].astype(F32)

        @pl.when(k >= 2)
        def _():
            out_copy(k - 2).wait()

        obuf[k % 2] = total.astype(BF16)
        out_copy(k).start()

    def out_step(k, _):
        for i in range(n_sp):
            @pl.when(k == i)
            def _():
                j = (i + 1) // 2
                if i == 0:
                    ring.tick(done_in + 0.28)
                elif j < hops:
                    ring.need(("out", 0, 0, j))
                    ring.need(("out", 1, 0, j))
                else:
                    ring.need(("out", 0, 0, j))

        stage_one(k)
        stage_two(k)

        @pl.when(k >= 1)
        def _():
            stage_three(k - 1)

        return 0

    lax.fori_loop(0, n_sp, out_step, 0)
    stage_three(n_sp - 1)
    ring.close()
    for k in range(max(0, n_sp - 2), n_sp):
        core_copy(k).wait_send()
        out_copy(k).wait()

    def drain(k, _):
        for d in range(1, n_y):
            y_copy(k, d).wait_send()
        return 0

    lax.fori_loop(0, n_sp, drain, 0)

    halo_leave(POOL)
    for r in range(n_round):
        @pl.when(sp + shifts[r] < n_sp)
        def _():
            scan_copy(r, sources[r]).wait_send()


def pool_mix(cfg, raw, gmw, cscale_ref, sp, tp, tile, rows, width):
    groups = gmw.shape[0]

    def body(t, _):
        window = pl.ds(pl.multiple_of(t * tile, tile), tile + PAD)
        to = pl.ds(pl.multiple_of(PAD + t * tile, PAD), tile)
        place = sp * rows + t * tile + lax.broadcasted_iota(jnp.int32, (tile, 1), 0) + 1
        for g in range(groups):
            cols = slice(g * GROUP_DIM, (g + 1) * GROUP_DIM)
            extended = raw[POOL, window, cols].astype(F32)
            sums = extended
            options = []
            for lag in (1, 2, 4, 8):
                sums = sums + pltpu.roll(sums, lag, 0)
                options.append(sums[PAD:])
            if groups % 4 == 0:
                size = 2 << (g % 4)
                windowed = options[g % 4]
            else:
                which = (tp * groups + g) % 4
                size = jnp.where(which == 0, 2, jnp.where(which == 1, 4, jnp.where(which == 2, 8, 16)))
                windowed = options[3]
                for i in range(3):
                    windowed = jnp.where(which == i, options[i], windowed)
            counts = jnp.minimum(place, size).astype(F32)
            diff = (windowed / counts - extended[PAD:]).astype(BF16)
            mixed = jnp.dot(diff, gmw[g], preferred_element_type=F32)
            scale = cscale_ref[:, pl.ds(pl.multiple_of(tp * width + g * GROUP_DIM, 128), GROUP_DIM)]
            raw[KEY, to, cols] = (mixed * scale.astype(F32)).astype(BF16)
        return 0

    lax.fori_loop(0, rows // tile, body, 0)


def per_device(
    n_sp,
    n_tp,
    tokens,
    input_norm_scale,
    mean_input_weight,
    query_matrix,
    key_matrix,
    value_matrix,
    strength_weight,
    decay_input_weight,
    causal_filter_weight,
    head_decay_logrates,
    decay_input_shift,
    strength_shift,
    decay_spike,
    head_norm_scale,
    group_mixing_weight,
    mean_channel_scale,
    mean_output_weight,
    delta_output_weight,
):
    rows, dim = tokens.shape
    rows_in, width = key_matrix.shape
    heads = strength_weight.shape[1]
    depth = width // heads
    rows_out, cols_out = mean_output_weight.shape
    n_y = n_tp // 2
    share = rows // n_tp
    groups = mean_input_weight.shape[1] // GROUP_DIM
    hops = n_sp // 2
    grid_x = 1
    while grid_x * grid_x * 4 <= n_sp:
        grid_x *= 2
    narrow = jnp.concatenate([strength_weight, decay_input_weight], axis=1).T
    narrow = jnp.pad(narrow, ((0, PAD - 2 * heads), (0, width - rows_in)))
    n_items = 3 * hops + 2 * (2 * hops - 1)
    n_round = 2
    while 2 ** (n_round - 1) < n_sp - 1:
        n_round += 1
    any_ = pl.BlockSpec(memory_space=pl.ANY)
    vmem = pl.BlockSpec(memory_space=pltpu.VMEM)
    dma = pltpu.SemaphoreType.DMA
    return pl.pallas_call(
        lambda *refs: mixer_kernel((n_sp, n_tp, heads, depth, grid_x), *refs),
        out_shape=jax.ShapeDtypeStruct((share, dim), BF16),
        in_specs=[any_, vmem, any_, any_, any_, any_, any_]
        + [vmem] * 6
        + [any_, vmem, any_, any_],
        out_specs=any_,
        scratch_shapes=[
            pltpu.VMEM((4, n_sp, rows_in + PAD, width), BF16),
            pltpu.VMEM((2, n_sp, rows_out, cols_out), BF16),
            pltpu.VMEM((n_sp, rows, rows_in), BF16),
            pltpu.VMEM((4, rows, width), F32),
            pltpu.VMEM((4, rows + PAD, width), BF16),
            pltpu.VMEM((2, min(128, rows), dim), BF16),
            pltpu.VMEM((rows, PAD), F32),
            pltpu.VMEM((groups, GROUP_DIM, GROUP_DIM), BF16),
            pltpu.VMEM((heads, depth, 2 * depth), F32),
            pltpu.VMEM((n_round, heads, depth, 2 * depth), BF16),
            pltpu.VMEM((n_round, heads, depth, 2 * depth), BF16),
            pltpu.VMEM((2, n_y, share, cols_out), BF16),
            pltpu.VMEM((n_sp, n_y, share, cols_out), BF16),
            pltpu.VMEM((n_sp, n_y - 1, share, cols_out), BF16),
            pltpu.VMEM((n_sp, n_y - 1, share, cols_out), BF16),
            pltpu.VMEM((2, share, cols_out), BF16),
            dma((n_items, 2)),
            dma((n_items, 2)),
            dma((8,)),
            dma((2,)),
            dma((4,)),
            dma((4,)),
            dma((n_round,)),
            dma((n_round,)),
            dma((n_sp,)),
            dma((n_sp,)),
            dma((n_sp, n_y - 1)),
            dma((n_sp, n_y - 1)),
            dma((2,)),
        ],
        compiler_params=pltpu.CompilerParams(
            collective_id=0, has_side_effects=True, vmem_limit_bytes=67043328
        ),
    )(
        tokens,
        input_norm_scale.reshape(1, dim),
        key_matrix,
        value_matrix,
        query_matrix,
        mean_input_weight,
        narrow,
        causal_filter_weight,
        head_decay_logrates.reshape(1, -1),
        decay_input_shift.reshape(1, -1),
        strength_shift.reshape(1, -1),
        decay_spike,
        head_norm_scale.reshape(1, -1),
        group_mixing_weight,
        mean_channel_scale.reshape(1, -1),
        mean_output_weight,
        delta_output_weight,
    )


def solution(mesh):
    n_sp, n_tp = mesh.shape["sp"], mesh.shape["tp"]
    return jax.shard_map(
        lambda *args: per_device(n_sp, n_tp, *args),
        mesh=mesh,
        in_specs=(
            P("sp", None),
            P(),
            P("sp", "tp"),
            P("sp", "tp"),
            P("sp", "tp"),
            P("sp", "tp"),
            P("sp", "tp"),
            P("sp", "tp"),
            P(),
            P(),
            P(),
            P(),
            P("sp", "tp"),
            P(),
            P(),
            P(),
            P("tp", "sp"),
            P("tp", "sp"),
        ),
        out_specs=P(("sp", "tp"), None),
        check_vma=False,
    )
```

time: 565 us -> 298 us (0.53)
  waiting for transfers between devices: 381 us -> 0 us
  Pallas kernels: 28.7 us -> 287 us
  matrix products: 65.1 us -> 0 us
  blocking collectives: 26.7 us -> 0 us
  starting transfers between devices: 20.8 us -> 0 us
  other arithmetic: 19 us -> 0.71 us
  between operations: 13.9 us -> 0.01 us
    all_gather x6 -> x0, waiting for transfers between devices: 280 us -> none  [the longest x4 179 us: per_device(): gather = lambda weight: lax.all_gather(weight, 'sp', axis=0, tiled=True)]
    pallas_call x2 -> x1, Pallas kernels: 28.7 us -> 287 us  [per_device(): pl.pallas_call(lambda *refs: mixer_kernel((n_sp, n_tp, heads, depth, grid...]
    reduce_scatter x1 -> x0, waiting for transfers between devices: 69.7 us -> none  [per_device(): lax.psum_scatter(jnp.dot(mixed, out_weight, preferred_element_type=jnp.fl...]
    dot_general x10 -> x0, matrix products: 65.1 us -> none  [the longest x5 42 us: per_device(): jnp.dot(normed, weight, preferred_element_type=F32).astype(BF16)]
    ppermute x8 -> x0, waiting for transfers between devices: 27.6 us -> none  [shifted_2(): return lax.ppermute(block, axis, route)]
    all_gather x1 -> x0, blocking collectives: 26.7 us -> none  [per_device(): lax.all_gather(jnp.concatenate([strength_weight, decay_input_weight], axi...]
    ppermute x8 -> x0, starting transfers between devices: 20.6 us -> none  [shifted_2(): return lax.ppermute(block, axis, route)]
    convert_element_type x6 -> x0, other arithmetic: 13.1 us -> none  [the longest x1 10.7 us: per_device(): scale_rows(tokens.astype(jnp.float32), input_norm_scale)]
  transfers between devices with their start and end apart: 15 -> 0, of which waited for: 11 -> 0; matrix products, arithmetic and copies ran while one was open for 13% -> 0% of each run, Pallas kernels for 5% -> 0%
where the time goes in v1:
time: 298 us; the launch traced here: 297 us
  Pallas kernels  287 us (96%)
  local copies, waits for them, and re-layouts  9.52 us (3%)
    pallas_call x1, Pallas kernels, per_device(): pl.pallas_call(lambda *refs: mixer_kernel((n_sp, n_tp, heads, depth, grid...  287 us
    unnamed x3, local copies, waits for them, and re-layouts  6.32 us

profile of v1, /device:TPU:20, one launch (start us, length us, event | category | flops | bytes accessed | tf_op | source)
XLA Modules:
  0.0 297.0 jit_solution(16769475632035796760)
XLA Ops:
  0.0 0.7 maximum_bitcast_fusion
  0.7 0.6 pad.4.refs_6_
  1.3 1.3 reshape.23.refs_14_
  2.6 1.3 reshape.18.refs_1_
  3.9 1.5 copy.19.refs_7_
  5.4 1.7 copy.20.refs_11_
  7.1 286.7 %shard_map.172 = bf16[256,4096]{1,0:T(8,128)(2,1)} custom-call(bf16[1024,4096]{1,0:T(8,128)(2,1)} %refs_0_.1, bf16[1,4096]{1,0:T(2,128)(2,1)} %reshape.18.refs_1_, bf16[512,512]{1,0:T(8,128)(2,1)} %refs_2_.1, bf16[512,512]{1,0:T(8,128)(2,1)} %refs_3_.1, bf16[512,512]{1,0:T(8,128)(2,1)} %refs_4_.1, bf16[512,512]{1,0:T(8,128)(2,1)} %refs_5_.1, ...), custom_call_target="tpu_custom_call" | custom-call | tf_op jit(solution)/shard_map/pallas_call | solution.py:777
  293.8 3.1 %copy.22 = bf16[256,4096]{1,0:T(8,128)(2,1)} copy(bf16[256,4096]{1,0:T(8,128)(2,1)} %shard_map.172) | data formatting | bytes 4194304

commit v2 on v1

v2 whole, which is shorter than its diff:
```python
import jax
import jax.numpy as jnp
from jax import lax
from jax.experimental import pallas as pl
from jax.experimental.pallas import tpu as pltpu
from jax.sharding import PartitionSpec as P

GROUP_DIM = 128
CONV = 4
EPSILON = 1e-06
PAD = 16
CHUNK = 128
BF16 = jnp.bfloat16
F32 = jnp.float32
MESH = pl.DeviceIdType.MESH
STATE_PART = 0.12
LAST_SINGLE = 2
MIDDLE = 2
SPLIT = 2
QUERY_PART = 0.03
KEY, VAL, QRY, POOL = range(4)


def dot(left, right):
    return jnp.dot(left.astype(BF16), right.astype(BF16), preferred_element_type=F32)


def dot_nt(left, right):
    return lax.dot_general(
        left.astype(BF16),
        right.astype(BF16),
        (((1,), (1,)), ((), ())),
        preferred_element_type=F32,
    )


def dot_tn(left, right):
    return lax.dot_general(
        left.astype(BF16),
        right.astype(BF16),
        (((0,), (0,)), ((), ())),
        preferred_element_type=F32,
    )


def unit_rows(values):
    return values * lax.rsqrt(jnp.sum(values * values, axis=-1, keepdims=True) + EPSILON)


def convolve(extended, taps, chunk):
    extended = extended.astype(F32)
    total = jnp.zeros((chunk, extended.shape[1]), F32)
    for i in range(CONV):
        start = PAD - (CONV - 1) + i
        total = total + taps[i] * extended[start : start + chunk]
    return total / (1.0 + jnp.exp(-total))


def decay_weights(cum_cols, cum_rows, h, causal):
    spread = cum_cols[:, h : h + 1] - cum_rows[h : h + 1, :]
    return jnp.where(causal, jnp.exp(jnp.where(causal, spread, 0.0)), 0.0)


def state_chunk(heads, depth, chunk, convolved, beta, decay, carry):
    row = lax.broadcasted_iota(jnp.int32, (chunk, chunk), 0)
    col = lax.broadcasted_iota(jnp.int32, (chunk, chunk), 1)
    causal = row >= col
    strict = row > col
    eye = jnp.where(row == col, 1.0, 0.0)
    tri = jnp.where(causal, 1.0, 0.0)
    cum_cols = jnp.dot(tri, decay, preferred_element_type=F32, precision=lax.Precision.HIGHEST)
    cum_rows = lax.dot_general(
        decay,
        tri,
        (((0,), (1,)), ((), ())),
        preferred_element_type=F32,
        precision=lax.Precision.HIGHEST,
    )
    base = min(16, chunk)
    hs = range(heads)
    k = [unit_rows(convolved[0][:, h * depth : (h + 1) * depth]) for h in hs]
    v = [convolved[1][:, h * depth : (h + 1) * depth] for h in hs]
    cum = [cum_cols[:, h : h + 1] for h in hs]
    last = [cum_cols[chunk - 1 : chunk, h : h + 1] for h in hs]
    beta = [beta[:, h : h + 1] for h in hs]
    weights = [decay_weights(cum_cols, cum_rows, h, causal) for h in hs]
    kb = [k[h] * beta[h] for h in hs]
    lower = [jnp.where(strict, dot_nt(kb[h], k[h]) * weights[h], 0.0) for h in hs]
    power = [jnp.where(row // base == col // base, lower[h], 0.0) for h in hs]
    inverse = [eye - power[h] for h in hs]
    reach = 2
    while reach < base:
        power = [dot(power[h], power[h]) for h in hs]
        inverse = [inverse[h] + dot(inverse[h], power[h]) for h in hs]
        reach *= 2
    size = base
    while size < chunk:
        pair = (row // (2 * size) == col // (2 * size)) & (row // size != col // size)
        right = [dot(jnp.where(pair, lower[h], 0.0), inverse[h]) for h in hs]
        inverse = [inverse[h] - dot(inverse[h], right[h]) for h in hs]
        size *= 2
    grow = [jnp.exp(cum[h]) for h in hs]
    sides = [jnp.concatenate([v[h] * beta[h], kb[h] * grow[h]], axis=1) for h in hs]
    solved = [dot(inverse[h], sides[h]) for h in hs]
    kd = [k[h] * jnp.exp(last[h] - cum[h]) for h in hs]
    zeros = jnp.zeros((chunk, depth), F32)
    state = [carry[h] for h in hs]
    fresh = [
        jnp.concatenate([solved[h][:, :depth], zeros], axis=1) - dot(solved[h][:, depth:], state[h])
        for h in hs
    ]
    for h in hs:
        carry[h] = state[h] * jnp.exp(last[h]) + dot_tn(kd[h], fresh[h])
    return k, cum_cols, cum_rows, state, fresh


class Ring:
    def __init__(self, hops, split, half_rows, refs, sems, owner, peers, window):
        self.refs, self.sems, self.owner, self.peers, self.window = refs, sems, owner, peers, window
        self.items = []
        self.index = {}
        rows_in, rows_out = half_rows
        top = rows_in // 2
        for j in range(1, hops + 1):
            for m in (KEY, VAL):
                full = rows_in + PAD if m == KEY else rows_in
                if j < hops:
                    self.add(("in", m, 0), j, [("in", m, 0, full)] * 2)
                else:
                    self.add(("in", m, 0), j, [("in", m, 0, top), ("in", m, top, full)])
        for j in range(1, hops + 1):
            for m in (QRY, POOL):
                if j < hops:
                    self.add(("in", m, 0), j, [("in", m, 0, top)] * 2)
                    self.add(("in", m, 1), j, [("in", m, top, rows_in)] * 2)
                else:
                    self.add(("in", m, 0), j, [("in", m, 0, top), ("in", m, top, rows_in)])
        for j in range(1, hops + 1):
            for e in range(split if j < hops else split // 2):
                other = e if j < hops else split // 2 + e
                self.add(("out", e, 0), j, [("out", e, 0, rows_out), ("out", other, 0, rows_out)])
        self.finish = []
        total = 0
        for _, _, parts in self.items:
            total += (parts[0][3] - parts[0][2]) * refs[parts[0][0]].shape[3]
            self.finish.append(total)
        self.total = total
        self.started = 0
        self.sent = set()
        self.received = set()

    def add(self, key, j, parts):
        self.index[key + (j,)] = len(self.items)
        self.items.append((key, j, parts))

    def copy(self, i, side):
        key, j, parts = self.items[i]
        kind, m, low, high = parts[side]
        ref = self.refs[kind]
        block = ref.at[m, self.owner(-(j - 1) if side == 0 else j - 1), pl.ds(low, high - low), :]
        return pltpu.make_async_remote_copy(
            src_ref=block,
            dst_ref=block,
            send_sem=self.sems[0].at[i, side],
            recv_sem=self.sems[1].at[i, side],
            device_id=self.peers[side],
            device_id_type=MESH,
        )

    def arrive(self, i, side):
        if (i, side) in self.received:
            return
        self.received.add((i, side))
        self.copy(i, side).wait_recv()

    def leave(self, i):
        if i in self.sent:
            return
        self.sent.add(i)
        for side in range(2):
            self.copy(i, side).wait_send()

    def start_next(self):
        i = self.started
        if i >= len(self.items):
            return
        behind = i - self.ahead(i)
        if behind >= 0:
            self.leave(behind)
        key, j, parts = self.items[i]
        for side in range(2):
            if j > 1:
                kind, m, low, high = parts[side]
                for before in range(i):
                    other, hop, pieces = self.items[before]
                    if hop == j - 1 and pieces[side][:2] == (kind, m) and pieces[side][2] <= low < pieces[side][3]:
                        self.arrive(before, side)
                    elif hop == j - 1 and pieces[side][:2] == (kind, m) and low <= pieces[side][2] < high:
                        self.arrive(before, side)
            self.copy(i, side).start()
        self.started += 1

    def ahead(self, i):
        if i >= len(self.items) - LAST_SINGLE:
            return 1
        return MIDDLE if self.items[i][0][1] in (QRY, POOL) and self.items[i][0][0] == "in" else 2

    def tick(self, part):
        while self.started < len(self.items):
            behind = self.started - self.ahead(self.started)
            if behind >= 0 and self.finish[behind] > part * self.total:
                break
            self.start_next()

    def need(self, key):
        i = self.index[key]
        while self.started < len(self.items) and self.started - self.ahead(self.started) <= i:
            self.start_next()
        for side in range(2):
            self.arrive(i, side)

    def close(self):
        while self.started < len(self.items):
            self.start_next()
        for i in range(len(self.items)):
            for side in range(2):
                self.arrive(i, side)
            self.leave(i)


def mixer_kernel(cfg, *refs):
    (
        tok_ref, gain_ref, wk_ref, wv_ref, wq_ref, wp_ref, strength_ref, slow_ref, tap_ref, rate_ref,
        dshift_ref, sshift_ref, spike_ref, hgain_ref, gmw_ref, cscale_ref, wpo_ref, wdo_ref,
    ) = refs[:18]
    out_ref = refs[18]
    (
        win, wout, normed, acc, raw, stage, before_tok, nraw, rowcum, tail, gain, cscale, gmw, carry, held,
        caught, psend, corerecv, ysend, yrecv, obuf, ring_send, ring_recv, local_sem, tok_sem, halo_sem,
        scan_send, scan_recv, core_send, core_recv, y_send, y_recv, out_sem,
    ) = refs[19:]
    n_sp, n_tp, heads, depth, grid_x = cfg
    grid_z = n_sp // grid_x
    hops = n_sp // 2
    n_y = n_tp // 2
    rows, width = raw.shape[1] - PAD, raw.shape[2]
    rows_in = normed.shape[2]
    split, rows_out, cols_half = wout.shape[0], wout.shape[2] // 2, wout.shape[3]
    share = rows // n_tp
    sp = lax.axis_index("sp")
    tp = lax.axis_index("tp")
    core = tp % 2
    ypos = tp // 2

    def sp_at(r):
        s = jnp.maximum(r - grid_z, 0)
        i = s // (grid_x - 1)
        k = s % (grid_x - 1)
        x = 1 + jnp.where(i % 2 == 0, k, grid_x - 2 - k)
        return jnp.where(r < grid_z, r * grid_x, (grid_z - 1 - i) * grid_x + x)

    zc = sp // grid_x
    xc = sp % grid_x
    ic = grid_z - 1 - zc
    kc = jnp.where(ic % 2 == 0, xc - 1, grid_x - 1 - xc)
    pos = jnp.where(xc == 0, zc, grid_z + ic * (grid_x - 1) + kc)

    def owner(offset):
        return sp_at((pos + offset + n_sp) % n_sp)

    barrier = pltpu.get_barrier_semaphore()
    for k in range(1, n_sp):
        pl.semaphore_signal(barrier, inc=1, device_id=((sp + k) % n_sp, tp), device_id_type=MESH)
    for k in range(1, n_tp):
        pl.semaphore_signal(barrier, inc=1, device_id=(sp, (tp + k) % n_tp), device_id_type=MESH)

    locals_ = []

    def bring(src, dst):
        locals_.append(pltpu.make_async_copy(src, dst, local_sem.at[len(locals_)]))
        locals_[-1].start()

    groups = gmw.shape[0]
    bring(wk_ref, win.at[KEY, sp, pl.ds(0, rows_in), :])
    bring(wv_ref, win.at[VAL, sp, pl.ds(0, rows_in), :])
    bring(wq_ref, win.at[QRY, sp, pl.ds(0, rows_in), :])
    bring(wp_ref, win.at[POOL, sp, pl.ds(0, rows_in), :])
    for half in range(split):
        cols = pl.ds(half * cols_half, cols_half)
        bring(wpo_ref.at[:, cols], wout.at[half, sp, pl.ds(0, rows_out), :])
        bring(wdo_ref.at[:, cols], wout.at[half, sp, pl.ds(rows_out, rows_out), :])
    bring(gmw_ref.at[pl.ds(tp * groups, groups)], gmw)
    step_rows = stage.shape[1]
    n_stage = rows // step_rows

    def token_copy(t, slot):
        return pltpu.make_async_copy(
            tok_ref.at[pl.ds(pl.multiple_of(t * step_rows, step_rows), step_rows), :],
            stage.at[slot],
            tok_sem.at[slot],
        )

    token_copy(0, 0).start()
    win[KEY, sp, pl.ds(rows_in, PAD), pl.ds(0, rows_in)] = jnp.concatenate(
        [
            strength_ref[...].astype(F32),
            slow_ref[...].astype(F32),
            jnp.zeros((PAD - 2 * heads, rows_in), F32),
        ],
        axis=0,
    ).astype(BF16)
    for i in range(gain_ref.shape[0]):
        gain[:, i * 128 : (i + 1) * 128] = gain_ref[i : i + 1, :].astype(F32)
    cscale[...] = cscale_ref[...].astype(F32)
    locals_[0].wait()
    locals_[1].wait()
    pl.semaphore_wait(barrier, n_sp + n_tp - 2)

    halo = pltpu.make_async_remote_copy(
        src_ref=tok_ref.at[pl.ds(rows - PAD, PAD), :],
        dst_ref=before_tok,
        send_sem=halo_sem.at[0],
        recv_sem=halo_sem.at[1],
        device_id=((sp + 1) % n_sp, tp),
        device_id_type=MESH,
    )

    @pl.when(sp + 1 < n_sp)
    def _():
        halo.start()

    ring = Ring(
        hops,
        split,
        (rows_in, wout.shape[2]),
        {"in": win, "out": wout},
        (ring_send, ring_recv),
        owner,
        [(owner(1), tp), (owner(-1), tp)],
        2,
    )
    ring.tick(0.0)
    for c in locals_[2:]:
        c.wait()

    def norm_rows(load, to, count):
        squares = jnp.zeros((count, 1), F32)
        for b in range(n_sp):
            x = load(slice(b * rows_in, (b + 1) * rows_in)).astype(F32)
            squares = squares + jnp.sum(x * x, axis=-1, keepdims=True)
        scale = lax.rsqrt(squares * (1.0 / (n_sp * rows_in)) + EPSILON)
        for b in range(n_sp):
            cols = slice(b * rows_in, (b + 1) * rows_in)
            normed[b, to, :] = (load(cols).astype(F32) * scale * gain[:, cols]).astype(BF16)

    def norm_step(t, _):
        slot = t % 2
        token_copy(t, slot).wait()

        @pl.when(t + 1 < n_stage)
        def _():
            token_copy(t + 1, 1 - slot).start()

        def piece(u, _):
            at = pl.ds(pl.multiple_of(u * 32, 32), 32)
            to = pl.ds(pl.multiple_of(PAD + t * step_rows + u * 32, PAD), 32)
            norm_rows(lambda cols: stage[slot, at, cols], to, 32)
            return 0

        lax.fori_loop(0, step_rows // 32, piece, 0)
        return 0

    lax.fori_loop(0, n_stage, norm_step, 0)

    @pl.when(sp > 0)
    def _():
        halo.wait_recv()

    @pl.when(sp == 0)
    def _():
        before_tok[...] = jnp.zeros(before_tok.shape, BF16)

    norm_rows(lambda cols: before_tok[:, cols], pl.ds(0, PAD), PAD)

    tile = max(d for d in range(PAD, 273, PAD) if (rows + PAD) % d == 0)
    n_tile = (rows + PAD) // tile

    def project(m, owners, first=False, final=False):
        def body(t, _):
            at = pl.ds(pl.multiple_of(t * tile, PAD), tile)
            total = None if first else acc[m, at, :]
            for o in owners:
                term = jnp.dot(
                    normed[o, at, :], win[m, o, pl.ds(0, rows_in), :], preferred_element_type=F32
                )
                total = term if total is None else total + term
            if final:
                raw[m, at, :] = total.astype(BF16)
            else:
                acc[m, at, :] = total
            return 0

        lax.fori_loop(0, n_tile, body, 0)

    def own(m, _):
        project(m, [sp], first=True)
        return 0

    lax.fori_loop(0, 4, own, 0)

    def arriving(i, _):
        for k in range(2 * hops):
            @pl.when(i == k)
            def _():
                ring.need(("in", k % 2, 0, k // 2 + 1))

        m, j = i % 2, i // 2 + 1

        @pl.when(j < hops)
        def _():
            project(m, [owner(-j), owner(j)])

        @pl.when(j == hops)
        def _():
            project(m, [owner(hops)], final=True)

        return 0

    lax.fori_loop(0, 2 * hops, arriving, 0)
    block = min(256, rows)
    n_block = rows // block

    def narrow_body(t, _):
        at = pl.ds(pl.multiple_of(t * block, block), block)
        total = jnp.zeros((block, PAD), F32)
        for o in range(n_sp):
            total = total + dot_nt(
                normed[o, pl.ds(pl.multiple_of(PAD + t * block, PAD), block), :],
                win[KEY, o, pl.ds(rows_in, PAD), pl.ds(0, rows_in)],
            )
        nraw[at, :] = total
        return 0

    lax.fori_loop(0, n_block, narrow_body, 0)

    lane = lax.broadcasted_iota(jnp.int32, (1, rate_ref.shape[1]), 1)
    small = lax.broadcasted_iota(jnp.int32, (1, heads), 1)

    def head_row(ref):
        total = jnp.zeros((1, heads), F32)
        for h in range(heads):
            value = jnp.sum(jnp.where(lane == tp * heads + h, ref[...], 0.0), axis=-1, keepdims=True)
            total = total + jnp.where(small == h, value, 0.0)
        return total

    speed = -jnp.exp(head_row(rate_ref))
    dshift = head_row(dshift_ref)
    sshift = head_row(sshift_ref)
    mine = pl.ds(pl.multiple_of(tp * width, 128), width)
    wide = lax.broadcasted_iota(jnp.int32, (depth, 2 * depth), 1)
    sub = lax.broadcasted_iota(jnp.int32, (depth, 2 * depth), 0)
    for h in range(heads):
        carry[h] = jnp.where(wide == sub + depth, 1.0, 0.0)
    chunk = min(CHUNK, rows)
    n_chunk = rows // chunk
    tail[...] = raw[KEY, pl.ds(0, PAD), :]
    one = lax.broadcasted_iota(jnp.int32, (heads, heads), 0) == lax.broadcasted_iota(
        jnp.int32, (heads, heads), 1
    )
    per_slot = stage.shape[2] // (2 * depth)
    fresh_at = [((h * 2 * depth) // width, (h * 2 * depth) % width) for h in range(heads)]

    def stage_at(c, h):
        flat = c * heads + h
        cols = pl.ds(pl.multiple_of((flat % per_slot) * 2 * depth, 128), 2 * depth)
        return stage.at[flat // per_slot, pl.ds(0, depth), cols]

    third = 1.0 / 3.0

    def state_step(c, _):
        for k in range(n_chunk):
            @pl.when(c == k)
            def _():
                ring.tick(third + STATE_PART * k / n_chunk)

        at = pl.ds(pl.multiple_of(c * chunk, chunk), chunk)
        to = pl.ds(pl.multiple_of(PAD + c * chunk, PAD), chunk)
        window = pl.ds(pl.multiple_of(c * chunk, chunk), chunk + PAD)
        keys = jnp.concatenate([tail[...], raw[KEY, to, :]], axis=0)
        tail[...] = keys[chunk:]
        taps = [[tap_ref[r, i : i + 1, mine].astype(F32) for i in range(CONV)] for r in range(3)]
        convolved = [convolve(keys, taps[1], chunk), convolve(raw[VAL, window, :], taps[2], chunk)]
        narrow = nraw[at, :].astype(BF16).astype(F32)
        beta = 1.0 / (1.0 + jnp.exp(-(narrow[:, :heads] + sshift)))
        x = narrow[:, heads : 2 * heads] + dshift
        soft = jnp.maximum(x, 0.0) + jnp.log1p(jnp.exp(-jnp.abs(x)))
        spike = lax.dot_general(
            spike_ref[:, at],
            jnp.where(one, 1.0, 0.0),
            (((0,), (0,)), ((), ())),
            preferred_element_type=F32,
            precision=lax.Precision.HIGHEST,
        )
        decay = speed * soft + spike
        k, cum_cols, cum_rows, state, fresh = state_chunk(
            heads, depth, chunk, convolved, beta, decay, carry
        )
        nraw[at, pl.ds(0, heads)] = cum_cols
        rowcum[c] = cum_rows
        for h in range(heads):
            raw[KEY, to, h * depth : (h + 1) * depth] = k[h].astype(BF16)
            stage_at(c, h)[...] = state[h].astype(BF16)
            slot, low = fresh_at[h]
            acc[slot, at, low : low + 2 * depth] = fresh[h]
        return 0

    lax.fori_loop(0, n_chunk, state_step, 0)

    far = grid_x - 1
    whole, front = pl.ds(0, 2 * depth), pl.ds(0, depth)

    def pass_state(slot, source, target, pick, z, x):
        return pltpu.make_async_remote_copy(
            src_ref=source.at[:, :, pick],
            dst_ref=caught.at[target, :, :, pick],
            send_sem=scan_send.at[slot],
            recv_sem=scan_recv.at[target],
            device_id=(z * grid_x + x, tp),
            device_id_type=MESH,
        )

    along_x = pass_state(0, held.at[0], 0, whole, zc, (xc + 1) % grid_x)
    along_z = pass_state(1, held.at[1], 1, front, (zc + 1) % grid_z, xc)
    back = [
        pass_state(2 + x, caught.at[1], 2, front, zc, (xc + 1 + x) % grid_x) for x in range(far)
    ]

    @pl.when(xc == 0)
    def _():
        for h in range(heads):
            held[0, h] = carry[h].astype(BF16)
            caught[0, h] = jnp.where(wide == sub + depth, 1.0, 0.0).astype(BF16)
        along_x.start()

    def x_stage(x):
        @pl.when(xc == x)
        def _():
            along_x.wait_recv()
            for h in range(heads):
                later = carry[h]
                pushed = dot(later[:, depth:], caught[0, h])
                held[0, h, :, front] = (later[:, :depth] + pushed[:, :depth]).astype(BF16)
                held[0, h, :, pl.ds(depth, depth)] = pushed[:, depth:].astype(BF16)
            if x < far:
                along_x.start()

    def z_stage(z):
        @pl.when((xc == far) & (zc == z))
        def _():
            if z == 0:
                for h in range(heads):
                    caught[1, h, :, front] = jnp.zeros((depth, depth), BF16)
            else:
                along_z.wait_recv()
                for c in back:
                    c.start()
            if z + 1 < grid_z:
                for h in range(heads):
                    later = held[0, h]
                    pushed = dot(later[:, depth:], caught[1, h, :, front])
                    held[1, h, :, front] = (later[:, :depth].astype(F32) + pushed).astype(BF16)
                along_z.start()

    def last_stage():
        @pl.when((xc < far) & (zc > 0))
        def _():
            back[0].wait_recv()
            for h in range(heads):
                caught[1, h, :, front] = caught[2, h, :, front]

        @pl.when((xc < far) & (zc == 0))
        def _():
            for h in range(heads):
                caught[1, h, :, front] = jnp.zeros((depth, depth), BF16)

        for h in range(heads):
            later = caught[0, h]
            pushed = dot(later[:, depth:], caught[1, h, :, front])
            held[2, h, :, front] = (later[:, :depth].astype(F32) + pushed).astype(BF16)

    incoming = held.at[2]

    def hop(m, j):
        ring.need(("in", m, 0, j))
        if j < hops:
            ring.need(("in", m, 1, j))
            project(m, [owner(-j), owner(j)])
        else:
            project(m, [owner(hops)], final=True)

    steps = [(m, j) for j in range(1, hops + 1) for m in (QRY, POOL)][:-1]
    for i, (m, j) in enumerate(steps):
        hop(m, j)
        if 2 <= i <= far + 1:
            x_stage(i - 1)
        if far < i <= far + grid_z:
            z_stage(i - far - 1)
    last_stage()

    hgain = hgain_ref[...].astype(F32)
    row = lax.broadcasted_iota(jnp.int32, (chunk, chunk), 0)
    col = lax.broadcasted_iota(jnp.int32, (chunk, chunk), 1)
    causal = row >= col

    def query_step(c, _):
        for k in range(n_chunk):
            @pl.when(c == k)
            def _():
                ring.tick(2 * third - 0.02 + QUERY_PART * k / n_chunk)

        at = pl.ds(pl.multiple_of(c * chunk, chunk), chunk)
        to = pl.ds(pl.multiple_of(PAD + c * chunk, PAD), chunk)
        window = pl.ds(pl.multiple_of(c * chunk, chunk), chunk + PAD)
        taps = [tap_ref[0, i : i + 1, mine].astype(F32) for i in range(CONV)]
        convolved = convolve(raw[QRY, window, :], taps, chunk)
        cum_cols = nraw[at, :]
        cum_rows = rowcum[c]
        hs = range(heads)
        spans = [slice(h * depth, (h + 1) * depth) for h in hs]
        q = [unit_rows(convolved[:, spans[h]]) * depth ** (-0.5) for h in hs]
        weights = [decay_weights(cum_cols, cum_rows, h, causal) for h in hs]
        scores = [dot_nt(q[h], raw[KEY, to, spans[h]]) * weights[h] for h in hs]
        grow = [jnp.exp(cum_cols[:, h : h + 1]) for h in hs]
        outs = []
        for h in hs:
            slot, low = fresh_at[h]
            outs.append(
                dot(q[h] * grow[h], stage_at(c, h)[...])
                + dot(scores[h], acc[slot, at, low : low + 2 * depth])
            )
        values = [
            outs[h][:, :depth] + dot(outs[h][:, depth:], incoming[h, :, pl.ds(0, depth)]) for h in hs
        ]
        for h in hs:
            scale = lax.rsqrt(jnp.mean(values[h] * values[h], axis=-1, keepdims=True) + EPSILON)
            raw[VAL, to, spans[h]] = (values[h] * scale * hgain).astype(BF16)
        return 0

    lax.fori_loop(0, n_chunk, query_step, 0)
    hop(POOL, hops)
    pool_mix(cfg, raw, gmw, cscale, sp, tp, block, rows, width)

    n_pair = split * hops

    def half_of(p, u):
        q = jnp.maximum(p - split // 2, 0)
        t = p - (n_pair - split // 2)
        step = jnp.where(p < split // 2, 0, q // split + 1)
        part = jnp.where(
            p < split // 2, 2 * p + u, jnp.where(t >= 0, u * (split // 2) + t, q % split)
        )
        return owner((2 * u - 1) * step), part

    def partial(dest, o, half):
        at = pl.ds(pl.multiple_of(PAD + dest * share, PAD), share)
        total = jnp.dot(
            raw[KEY, at, :], wout[half, o, pl.ds(0, rows_out), :], preferred_element_type=F32
        ) + jnp.dot(
            raw[VAL, at, :], wout[half, o, pl.ds(rows_out, rows_out), :], preferred_element_type=F32
        )
        return total.astype(BF16)

    def core_copy(p):
        return pltpu.make_async_remote_copy(
            src_ref=psend.at[p % 2],
            dst_ref=corerecv.at[p],
            send_sem=core_send.at[p],
            recv_sem=core_recv.at[p],
            device_id=(sp, ypos * 2 + 1 - core),
            device_id_type=MESH,
        )

    def y_copy(p, d):
        return pltpu.make_async_remote_copy(
            src_ref=ysend.at[p, d - 1],
            dst_ref=yrecv.at[p, d - 1],
            send_sem=y_send.at[p, d - 1],
            recv_sem=y_recv.at[p, d - 1],
            device_id=(sp, ((ypos + d) % n_y) * 2 + core),
            device_id_type=MESH,
        )

    def out_copy(p, u):
        o, half = half_of(p, u)
        low = (o * split + half) * cols_half
        return pltpu.make_async_copy(
            obuf.at[p % 2, u],
            out_ref.at[:, pl.ds(pl.multiple_of(low, 128), cols_half)],
            out_sem.at[p % 2, u],
        )

    def own_at(p, u):
        at = pl.ds(pl.multiple_of((p % 4) * share, share), share)
        return acc.at[QRY, at, pl.ds(u * cols_half, cols_half)]

    def stage_one(p):
        @pl.when(p >= 2)
        def _():
            core_copy(p - 2).wait_send()

        for u in range(2):
            o, half = half_of(p, u)
            for y in range(n_y):
                psend[p % 2, y, u] = partial(y * 2 + 1 - core, o, half)
        core_copy(p).start()

    def stage_two(p):
        parts = []
        for u in range(2):
            o, half = half_of(p, u)
            parts.append([partial(((ypos + d) % n_y) * 2 + core, o, half) for d in range(n_y)])
        core_copy(p).wait_recv()
        for d in range(1, n_y):
            there = (ypos + d) % n_y
            for u in range(2):
                total = parts[u][d].astype(F32) + corerecv[p, there, u].astype(F32)
                ysend[p, d - 1, u] = total.astype(BF16)
            y_copy(p, d).start()
        for u in range(2):
            own_at(p, u)[...] = parts[u][0].astype(F32) + corerecv[p, ypos, u].astype(F32)

    def stage_three(p):
        for d in range(1, n_y):
            y_copy(p, d).wait_recv()
        for u in range(2):
            total = own_at(p, u)[...]
            for d in range(1, n_y):
                total = total + yrecv[p, d - 1, u].astype(F32)

            @pl.when(p >= 2)
            def _():
                out_copy(p - 2, u).wait()

            obuf[p % 2, u] = total.astype(BF16)
            out_copy(p, u).start()

    def out_step(p, _):
        for i in range(n_pair):
            @pl.when(p == i)
            def _():
                if i < split // 2:
                    ring.tick(2 * third)
                else:
                    e = i - split // 2
                    ring.need(("out", e % split, 0, e // split + 1))

        stage_one(p)

        @pl.when(p >= 2)
        def _():
            stage_three(p - 2)

        stage_two(p)
        return 0

    lax.fori_loop(0, n_pair, out_step, 0)
    stage_three(n_pair - 2)
    stage_three(n_pair - 1)
    ring.close()
    for p in range(n_pair - 2, n_pair):
        core_copy(p).wait_send()
        for u in range(2):
            out_copy(p, u).wait()

    def drain(p, _):
        for d in range(1, n_y):
            y_copy(p, d).wait_send()
        return 0

    lax.fori_loop(0, n_pair, drain, 0)

    @pl.when(sp + 1 < n_sp)
    def _():
        halo.wait_send()

    @pl.when(xc < far)
    def _():
        along_x.wait_send()

    @pl.when((xc == far) & (zc + 1 < grid_z))
    def _():
        along_z.wait_send()

    @pl.when((xc == far) & (zc > 0))
    def _():
        for c in back:
            c.wait_send()


def pool_mix(cfg, raw, gmw, cscale, sp, tp, tile, rows, width):
    groups = gmw.shape[0]

    def body(t, _):
        window = pl.ds(pl.multiple_of(t * tile, tile), tile + PAD)
        to = pl.ds(pl.multiple_of(PAD + t * tile, PAD), tile)
        place = sp * rows + t * tile + lax.broadcasted_iota(jnp.int32, (tile, 1), 0) + 1
        for g in range(groups):
            cols = slice(g * GROUP_DIM, (g + 1) * GROUP_DIM)
            extended = raw[POOL, window, cols].astype(F32)
            sums = extended
            options = []
            for lag in (1, 2, 4, 8):
                sums = sums + pltpu.roll(sums, lag, 0)
                options.append(sums[PAD:])
            if groups % 4 == 0:
                size = 2 << (g % 4)
                windowed = options[g % 4]
            else:
                which = (tp * groups + g) % 4
                size = jnp.where(which == 0, 2, jnp.where(which == 1, 4, jnp.where(which == 2, 8, 16)))
                windowed = options[3]
                for i in range(3):
                    windowed = jnp.where(which == i, options[i], windowed)
            counts = jnp.minimum(place, size).astype(F32)
            diff = (windowed / counts - extended[PAD:]).astype(BF16)
            mixed = jnp.dot(diff, gmw[g], preferred_element_type=F32)
            scale = cscale[pl.ds(tp * groups + g, 1), :]
            raw[KEY, to, cols] = (mixed * scale).astype(BF16)
        return 0

    lax.fori_loop(0, rows // tile, body, 0)


def per_device(
    n_sp,
    n_tp,
    tokens,
    input_norm_scale,
    mean_input_weight,
    query_matrix,
    key_matrix,
    value_matrix,
    strength_weight,
    decay_input_weight,
    causal_filter_weight,
    head_decay_logrates,
    decay_input_shift,
    strength_shift,
    decay_spike,
    head_norm_scale,
    group_mixing_weight,
    mean_channel_scale,
    mean_output_weight,
    delta_output_weight,
):
    rows, dim = tokens.shape
    rows_in, width = key_matrix.shape
    heads = strength_weight.shape[1]
    depth = width // heads
    rows_out, cols_out = mean_output_weight.shape
    n_y = n_tp // 2
    share = rows // n_tp
    groups = mean_input_weight.shape[1] // GROUP_DIM
    hops = n_sp // 2
    grid_x = 1
    while grid_x * grid_x * 4 <= n_sp:
        grid_x *= 2
    split = min(SPLIT, cols_out // 128)
    n_items = 2 * hops + 2 * (2 * (hops - 1) + 1) + split * (hops - 1) + split // 2
    any_ = pl.BlockSpec(memory_space=pl.ANY)
    vmem = pl.BlockSpec(memory_space=pltpu.VMEM)
    dma = pltpu.SemaphoreType.DMA
    return pl.pallas_call(
        lambda *refs: mixer_kernel((n_sp, n_tp, heads, depth, grid_x), *refs),
        out_shape=jax.ShapeDtypeStruct((share, dim), BF16),
        in_specs=[any_, vmem, any_, any_, any_, any_] + [vmem] * 8 + [any_, vmem, any_, any_],
        out_specs=any_,
        scratch_shapes=[
            pltpu.VMEM((4, n_sp, rows_in + PAD, width), BF16),
            pltpu.VMEM((split, n_sp, 2 * rows_out, cols_out // split), BF16),
            pltpu.VMEM((n_sp, rows + PAD, rows_in), BF16),
            pltpu.VMEM((4, rows + PAD, width), F32),
            pltpu.VMEM((4, rows + PAD, width), BF16),
            pltpu.VMEM((2, depth, dim), BF16),
            pltpu.VMEM((PAD, dim), BF16),
            pltpu.VMEM((rows, PAD), F32),
            pltpu.VMEM((rows // min(CHUNK, rows), heads, min(CHUNK, rows)), F32),
            pltpu.VMEM((PAD, width), BF16),
            pltpu.VMEM((1, dim), F32),
            pltpu.VMEM((mean_channel_scale.shape[0] // GROUP_DIM, GROUP_DIM), F32),
            pltpu.VMEM((groups, GROUP_DIM, GROUP_DIM), BF16),
            pltpu.VMEM((heads, depth, 2 * depth), F32),
            pltpu.VMEM((3, heads, depth, 2 * depth), BF16),
            pltpu.VMEM((3, heads, depth, 2 * depth), BF16),
            pltpu.VMEM((2, n_y, 2, share, cols_out // split), BF16),
            pltpu.VMEM((split * hops, n_y, 2, share, cols_out // split), BF16),
            pltpu.VMEM((split * hops, n_y - 1, 2, share, cols_out // split), BF16),
            pltpu.VMEM((split * hops, n_y - 1, 2, share, cols_out // split), BF16),
            pltpu.VMEM((2, 2, share, cols_out // split), BF16),
            dma((n_items, 2)),
            dma((n_items, 2)),
            dma((6 + 2 * split,)),
            dma((2,)),
            dma((2,)),
            dma((1 + grid_x,)),
            dma((3,)),
            dma((split * hops,)),
            dma((split * hops,)),
            dma((split * hops, n_y - 1)),
            dma((split * hops, n_y - 1)),
            dma((2, 2)),
        ],
        compiler_params=pltpu.CompilerParams(
            collective_id=0, has_side_effects=True, vmem_limit_bytes=64500000
        ),
    )(
        tokens,
        input_norm_scale.reshape(-1, 128),
        key_matrix,
        value_matrix,
        query_matrix,
        mean_input_weight,
        strength_weight.T,
        decay_input_weight.T,
        jnp.transpose(causal_filter_weight, (1, 0, 2)),
        head_decay_logrates.reshape(1, -1),
        decay_input_shift.reshape(1, -1),
        strength_shift.reshape(1, -1),
        decay_spike.T,
        head_norm_scale.reshape(1, -1),
        group_mixing_weight,
        mean_channel_scale.reshape(-1, GROUP_DIM),
        mean_output_weight,
        delta_output_weight,
    )


def solution(mesh):
    n_sp, n_tp = mesh.shape["sp"], mesh.shape["tp"]
    return jax.shard_map(
        lambda *args: per_device(n_sp, n_tp, *args),
        mesh=mesh,
        in_specs=(
            P("sp", None),
            P(),
            P("sp", "tp"),
            P("sp", "tp"),
            P("sp", "tp"),
            P("sp", "tp"),
            P("sp", "tp"),
            P("sp", "tp"),
            P(),
            P(),
            P(),
            P(),
            P("sp", "tp"),
            P(),
            P(),
            P(),
            P("tp", "sp"),
            P("tp", "sp"),
        ),
        out_specs=P(("sp", "tp"), None),
        check_vma=False,
    )
```

time: 298 us -> 268 us (0.90)
  Pallas kernels: 287 us -> 263 us
  local copies, waits for them, and re-layouts: 9.52 us -> 3.13 us
    pallas_call x1, Pallas kernels: 287 us -> 263 us  [per_device(): pl.pallas_call(lambda *refs: mixer_kernel((n_sp, n_tp, heads, depth, grid...]
    unnamed x3 -> x1, local copies, waits for them, and re-layouts: 6.32 us -> 3.13 us
where the time goes in v2:
time: 268 us; the launch traced here: 266 us
  Pallas kernels  263 us (98%)
  local copies, waits for them, and re-layouts  3.13 us (1%)
    pallas_call x1, Pallas kernels, per_device(): pl.pallas_call(lambda *refs: mixer_kernel((n_sp, n_tp, heads, depth, grid...  263 us

profile of v2, /device:TPU:20, one launch (start us, length us, event | category | flops | bytes accessed | tf_op | source)
XLA Modules:
  0.0 265.7 jit_solution(1586294858820331736)
XLA Ops:
  0.0 262.6 %shard_map.172 = bf16[256,4096]{1,0:T(8,128)(2,1)} custom-call(bf16[1024,4096]{1,0:T(8,128)(2,1)} %refs_0_.1, bf16[32,128]{1,0:T(8,128)(2,1)} %bitcast.12, bf16[512,512]{1,0:T(8,128)(2,1)} %refs_2_.1, bf16[512,512]{1,0:T(8,128)(2,1)} %refs_3_.1, bf16[512,512]{1,0:T(8,128)(2,1)} %refs_4_.1, bf16[512,512]{1,0:T(8,128)(2,1)} %refs_5_.1, ...), custom_call_target="tpu_custom_call" | custom-call | tf_op jit(solution)/shard_map/pallas_call | solution.py:873
  262.6 3.1 %copy.20 = bf16[256,4096]{1,0:T(8,128)(2,1)} copy(bf16[256,4096]{1,0:T(8,128)(2,1)} %shard_map.172) | data formatting | bytes 4194304

commit v3 on v2

--- a/solution.py
+++ b/solution.py
@@ -115,7 +115,7 @@
 
 
 class Ring:
-    def __init__(self, hops, split, half_rows, refs, sems, owner, peers, window):
+    def __init__(self, hops, split, subs, half_rows, refs, sems, owner, peers, window):
         self.refs, self.sems, self.owner, self.peers, self.window = refs, sems, owner, peers, window
         self.items = []
         self.index = {}
@@ -136,15 +136,23 @@
                 else:
                     self.add(("in", m, 0), j, [("in", m, 0, top), ("in", m, top, rows_in)])
         for j in range(1, hops + 1):
-            for e in range(split if j < hops else split // 2):
-                other = e if j < hops else split // 2 + e
-                self.add(("out", e, 0), j, [("out", e, 0, rows_out), ("out", other, 0, rows_out)])
+            if j < hops:
+                for e in range(split):
+                    self.add(("out", e, 0), j, [("out", e, 0, rows_out)] * 2)
+            else:
+                for e in range(split // 2):
+                    for c in range(subs):
+                        ends = [("out", e, 0, rows_out, c), ("out", split // 2 + e, 0, rows_out, c)]
+                        self.add(("out", e, c), j, ends)
         self.finish = []
         total = 0
         for _, _, parts in self.items:
-            total += (parts[0][3] - parts[0][2]) * refs[parts[0][0]].shape[3]
+            total += (parts[0][3] - parts[0][2]) * refs[parts[0][0]].shape[3] // (
+                subs if len(parts[0]) == 5 else 1
+            )
             self.finish.append(total)
         self.total = total
+        self.subs = subs
         self.started = 0
         self.sent = set()
         self.received = set()
@@ -155,9 +163,11 @@
 
     def copy(self, i, side):
         key, j, parts = self.items[i]
-        kind, m, low, high = parts[side]
+        kind, m, low, high = parts[side][:4]
         ref = self.refs[kind]
-        block = ref.at[m, self.owner(-(j - 1) if side == 0 else j - 1), pl.ds(low, high - low), :]
+        wide = ref.shape[3] // (self.subs if len(parts[side]) == 5 else 1)
+        cols = pl.ds(parts[side][4] * wide if len(parts[side]) == 5 else 0, wide)
+        block = ref.at[m, self.owner(-(j - 1) if side == 0 else j - 1), pl.ds(low, high - low), cols]
         return pltpu.make_async_remote_copy(
             src_ref=block,
             dst_ref=block,
@@ -190,7 +200,7 @@
         key, j, parts = self.items[i]
         for side in range(2):
             if j > 1:
-                kind, m, low, high = parts[side]
+                kind, m, low, high = parts[side][:4]
                 for before in range(i):
                     other, hop, pieces = self.items[before]
                     if hop == j - 1 and pieces[side][:2] == (kind, m) and pieces[side][2] <= low < pieces[side][3]:
@@ -239,7 +249,7 @@
         caught, psend, corerecv, ysend, yrecv, obuf, ring_send, ring_recv, local_sem, tok_sem, halo_sem,
         scan_send, scan_recv, core_send, core_recv, y_send, y_recv, out_sem,
     ) = refs[19:]
-    n_sp, n_tp, heads, depth, grid_x = cfg
+    n_sp, n_tp, heads, depth, grid_x, subs = cfg
     grid_z = n_sp // grid_x
     hops = n_sp // 2
     n_y = n_tp // 2
@@ -316,14 +326,27 @@
     locals_[1].wait()
     pl.semaphore_wait(barrier, n_sp + n_tp - 2)
 
+    part = tok_ref.shape[1] // n_tp
+    my_part = pl.ds(pl.multiple_of(tp * part, 128), part)
     halo = pltpu.make_async_remote_copy(
-        src_ref=tok_ref.at[pl.ds(rows - PAD, PAD), :],
-        dst_ref=before_tok,
-        send_sem=halo_sem.at[0],
-        recv_sem=halo_sem.at[1],
+        src_ref=tok_ref.at[pl.ds(rows - PAD, PAD), my_part],
+        dst_ref=before_tok.at[:, my_part],
+        send_sem=halo_sem.at[0, 0],
+        recv_sem=halo_sem.at[1, 0],
         device_id=((sp + 1) % n_sp, tp),
         device_id_type=MESH,
     )
+    spread = [
+        pltpu.make_async_remote_copy(
+            src_ref=before_tok.at[:, my_part],
+            dst_ref=before_tok.at[:, my_part],
+            send_sem=halo_sem.at[0, k],
+            recv_sem=halo_sem.at[1, k],
+            device_id=(sp, (tp + k) % n_tp),
+            device_id_type=MESH,
+        )
+        for k in range(1, n_tp)
+    ]
 
     @pl.when(sp + 1 < n_sp)
     def _():
@@ -332,6 +355,7 @@
     ring = Ring(
         hops,
         split,
+        subs,
         (rows_in, wout.shape[2]),
         {"in": win, "out": wout},
         (ring_send, ring_recv),
@@ -343,6 +367,12 @@
     for c in locals_[2:]:
         c.wait()
 
+    @pl.when(sp > 0)
+    def _():
+        halo.wait_recv()
+        for c in spread:
+            c.start()
+
     def norm_rows(load, to, count):
         squares = jnp.zeros((count, 1), F32)
         for b in range(n_sp):
@@ -374,7 +404,8 @@
 
     @pl.when(sp > 0)
     def _():
-        halo.wait_recv()
+        for c in spread:
+            c.wait_recv()
 
     @pl.when(sp == 0)
     def _():
@@ -661,91 +692,105 @@
         )
         return owner((2 * u - 1) * step), part
 
-    def partial(dest, o, half):
+    n_turn = n_pair - 1 + subs
+
+    def turn(b):
+        if isinstance(b, int) and b >= n_pair - 1 and subs > 1:
+            return n_pair - 1, (b - n_pair + 1) * (cols_half // subs), cols_half // subs
+        return b, 0, cols_half
+
+    def partial(dest, b, u):
+        p, low, wide_b = turn(b)
+        o, half = half_of(p, u)
         at = pl.ds(pl.multiple_of(PAD + dest * share, PAD), share)
+        cols = pl.ds(low, wide_b)
         total = jnp.dot(
-            raw[KEY, at, :], wout[half, o, pl.ds(0, rows_out), :], preferred_element_type=F32
+            raw[KEY, at, :], wout[half, o, pl.ds(0, rows_out), cols], preferred_element_type=F32
         ) + jnp.dot(
-            raw[VAL, at, :], wout[half, o, pl.ds(rows_out, rows_out), :], preferred_element_type=F32
+            raw[VAL, at, :], wout[half, o, pl.ds(rows_out, rows_out), cols], preferred_element_type=F32
         )
         return total.astype(BF16)
 
-    def core_copy(p):
+    def core_copy(b):
+        cols = pl.ds(0, turn(b)[2])
         return pltpu.make_async_remote_copy(
-            src_ref=psend.at[p % 2],
-            dst_ref=corerecv.at[p],
-            send_sem=core_send.at[p],
-            recv_sem=core_recv.at[p],
+            src_ref=psend.at[b % 2, :, :, :, cols],
+            dst_ref=corerecv.at[b, :, :, :, cols],
+            send_sem=core_send.at[b],
+            recv_sem=core_recv.at[b],
             device_id=(sp, ypos * 2 + 1 - core),
             device_id_type=MESH,
         )
 
-    def y_copy(p, d):
+    def y_copy(b, d):
+        cols = pl.ds(0, turn(b)[2])
         return pltpu.make_async_remote_copy(
-            src_ref=ysend.at[p, d - 1],
-            dst_ref=yrecv.at[p, d - 1],
-            send_sem=y_send.at[p, d - 1],
-            recv_sem=y_recv.at[p, d - 1],
+            src_ref=ysend.at[b, d - 1, :, :, cols],
+            dst_ref=yrecv.at[b, d - 1, :, :, cols],
+            send_sem=y_send.at[b, d - 1],
+            recv_sem=y_recv.at[b, d - 1],
             device_id=(sp, ((ypos + d) % n_y) * 2 + core),
             device_id_type=MESH,
         )
 
-    def out_copy(p, u):
+    def out_copy(b, u):
+        p, low, wide_b = turn(b)
         o, half = half_of(p, u)
-        low = (o * split + half) * cols_half
+        start = pl.multiple_of((o * split + half) * cols_half + low, 128)
         return pltpu.make_async_copy(
-            obuf.at[p % 2, u],
-            out_ref.at[:, pl.ds(pl.multiple_of(low, 128), cols_half)],
-            out_sem.at[p % 2, u],
+            obuf.at[b % 2, u, :, pl.ds(0, wide_b)],
+            out_ref.at[:, pl.ds(start, wide_b)],
+            out_sem.at[b % 2, u],
         )
 
-    def own_at(p, u):
-        at = pl.ds(pl.multiple_of((p % 4) * share, share), share)
-        return acc.at[QRY, at, pl.ds(u * cols_half, cols_half)]
-
-    def stage_one(p):
-        @pl.when(p >= 2)
+    def own_at(b, u):
+        at = pl.ds(pl.multiple_of((b % 4) * share, share), share)
+        return acc.at[QRY, at, pl.ds(u * cols_half, turn(b)[2])]
+
+    def stage_one(b):
+        @pl.when(b >= 2)
         def _():
-            core_copy(p - 2).wait_send()
-
+            core_copy(b - 2).wait_send()
+
+        cols = pl.ds(0, turn(b)[2])
         for u in range(2):
-            o, half = half_of(p, u)
             for y in range(n_y):
-                psend[p % 2, y, u] = partial(y * 2 + 1 - core, o, half)
-        core_copy(p).start()
-
-    def stage_two(p):
-        parts = []
-        for u in range(2):
-            o, half = half_of(p, u)
-            parts.append([partial(((ypos + d) % n_y) * 2 + core, o, half) for d in range(n_y)])
-        core_copy(p).wait_recv()
+                psend[b % 2, y, u, :, cols] = partial(y * 2 + 1 - core, b, u)
+        core_copy(b).start()
+
+    def stage_two(b):
+        cols = pl.ds(0, turn(b)[2])
+        parts = [
+            [partial(((ypos + d) % n_y) * 2 + core, b, u) for d in range(n_y)] for u in range(2)
+        ]
+        core_copy(b).wait_recv()
         for d in range(1, n_y):
             there = (ypos + d) % n_y
             for u in range(2):
-                total = parts[u][d].astype(F32) + corerecv[p, there, u].astype(F32)
-                ysend[p, d - 1, u] = total.astype(BF16)
-            y_copy(p, d).start()
+                total = parts[u][d].astype(F32) + corerecv[b, there, u, :, cols].astype(F32)
+                ysend[b, d - 1, u, :, cols] = total.astype(BF16)
+            y_copy(b, d).start()
         for u in range(2):
-            own_at(p, u)[...] = parts[u][0].astype(F32) + corerecv[p, ypos, u].astype(F32)
-
-    def stage_three(p):
+            own_at(b, u)[...] = parts[u][0].astype(F32) + corerecv[b, ypos, u, :, cols].astype(F32)
+
+    def stage_three(b):
+        cols = pl.ds(0, turn(b)[2])
         for d in range(1, n_y):
-            y_copy(p, d).wait_recv()
+            y_copy(b, d).wait_recv()
         for u in range(2):
-            total = own_at(p, u)[...]
+            total = own_at(b, u)[...]
             for d in range(1, n_y):
-                total = total + yrecv[p, d - 1, u].astype(F32)
-
-            @pl.when(p >= 2)
+                total = total + yrecv[b, d - 1, u, :, cols].astype(F32)
+
+            @pl.when(b >= 2)
             def _():
-                out_copy(p - 2, u).wait()
-
-            obuf[p % 2, u] = total.astype(BF16)
-            out_copy(p, u).start()
+                out_copy(b - 2, u).wait()
+
+            obuf[b % 2, u, :, cols] = total.astype(BF16)
+            out_copy(b, u).start()
 
     def out_step(p, _):
-        for i in range(n_pair):
+        for i in range(n_pair - 1):
             @pl.when(p == i)
             def _():
                 if i < split // 2:
@@ -763,25 +808,38 @@
         stage_two(p)
         return 0
 
-    lax.fori_loop(0, n_pair, out_step, 0)
-    stage_three(n_pair - 2)
-    stage_three(n_pair - 1)
+    lax.fori_loop(0, n_pair - 1, out_step, 0)
+    for c in range(subs):
+        ring.need(("out", split // 2 - 1, c, hops))
+        stage_one(n_pair - 1 + c)
+        if c == 0:
+            stage_three(n_pair - 3)
+        stage_two(n_pair - 1 + c)
+    for b in range(n_pair - 2, n_turn):
+        stage_three(b)
     ring.close()
-    for p in range(n_pair - 2, n_pair):
-        core_copy(p).wait_send()
+    for b in range(n_turn - 2, n_turn):
+        core_copy(b).wait_send()
         for u in range(2):
-            out_copy(p, u).wait()
-
-    def drain(p, _):
+            out_copy(b, u).wait()
+
+    def drain(b, _):
         for d in range(1, n_y):
-            y_copy(p, d).wait_send()
+            y_copy(b, d).wait_send()
         return 0
 
-    lax.fori_loop(0, n_pair, drain, 0)
+    lax.fori_loop(0, n_pair - 1, drain, 0)
+    for b in range(n_pair - 1, n_turn):
+        drain(b, 0)
 
     @pl.when(sp + 1 < n_sp)
     def _():
         halo.wait_send()
+
+    @pl.when(sp > 0)
+    def _():
+        for c in spread:
+            c.wait_send()
 
     @pl.when(xc < far)
     def _():
@@ -866,12 +924,14 @@
     while grid_x * grid_x * 4 <= n_sp:
         grid_x *= 2
     split = min(SPLIT, cols_out // 128)
-    n_items = 2 * hops + 2 * (2 * (hops - 1) + 1) + split * (hops - 1) + split // 2
+    subs = 2 if split == 2 and cols_out // split % 256 == 0 else 1
+    n_items = 2 * hops + 2 * (2 * (hops - 1) + 1) + split * (hops - 1) + split // 2 * subs
+    n_turn = split * hops - 1 + subs
     any_ = pl.BlockSpec(memory_space=pl.ANY)
     vmem = pl.BlockSpec(memory_space=pltpu.VMEM)
     dma = pltpu.SemaphoreType.DMA
     return pl.pallas_call(
-        lambda *refs: mixer_kernel((n_sp, n_tp, heads, depth, grid_x), *refs),
+        lambda *refs: mixer_kernel((n_sp, n_tp, heads, depth, grid_x, subs), *refs),
         out_shape=jax.ShapeDtypeStruct((share, dim), BF16),
         in_specs=[any_, vmem, any_, any_, any_, any_] + [vmem] * 8 + [any_, vmem, any_, any_],
         out_specs=any_,
@@ -893,25 +953,25 @@
             pltpu.VMEM((3, heads, depth, 2 * depth), BF16),
             pltpu.VMEM((3, heads, depth, 2 * depth), BF16),
             pltpu.VMEM((2, n_y, 2, share, cols_out // split), BF16),
-            pltpu.VMEM((split * hops, n_y, 2, share, cols_out // split), BF16),
-            pltpu.VMEM((split * hops, n_y - 1, 2, share, cols_out // split), BF16),
-            pltpu.VMEM((split * hops, n_y - 1, 2, share, cols_out // split), BF16),
+            pltpu.VMEM((n_turn, n_y, 2, share, cols_out // split), BF16),
+            pltpu.VMEM((n_turn, n_y - 1, 2, share, cols_out // split), BF16),
+            pltpu.VMEM((n_turn, n_y - 1, 2, share, cols_out // split), BF16),
             pltpu.VMEM((2, 2, share, cols_out // split), BF16),
             dma((n_items, 2)),
             dma((n_items, 2)),
             dma((6 + 2 * split,)),
             dma((2,)),
-            dma((2,)),
+            dma((2, n_tp)),
             dma((1 + grid_x,)),
             dma((3,)),
-            dma((split * hops,)),
-            dma((split * hops,)),
-            dma((split * hops, n_y - 1)),
-            dma((split * hops, n_y - 1)),
+            dma((n_turn,)),
+            dma((n_turn,)),
+            dma((n_turn, n_y - 1)),
+            dma((n_turn, n_y - 1)),
             dma((2, 2)),
         ],
         compiler_params=pltpu.CompilerParams(
-            collective_id=0, has_side_effects=True, vmem_limit_bytes=64500000
+            collective_id=0, has_side_effects=True, vmem_limit_bytes=67043328
         ),
     )(
         tokens,

time: 268 us -> 265 us (0.989)
  Pallas kernels: 263 us -> 258 us
    pallas_call x1, Pallas kernels: 263 us -> 258 us  [per_device(): pl.pallas_call(lambda *refs: mixer_kernel((n_sp, n_tp, heads, depth, grid...]
where the time goes in v3:
time: 265 us; the launch traced here: 261 us
  Pallas kernels  258 us (97%)
  local copies, waits for them, and re-layouts  3.13 us (1%)
    pallas_call x1, Pallas kernels, per_device(): pl.pallas_call(lambda *refs: mixer_kernel((n_sp, n_tp, heads, depth, grid...  258 us

profile of v3, /device:TPU:20, one launch (start us, length us, event | category | flops | bytes accessed | tf_op | source)
XLA Modules:
  0.0 261.0 jit_solution(10423747542338190896)
XLA Ops:
  0.0 257.9 %shard_map.172 = bf16[256,4096]{1,0:T(8,128)(2,1)} custom-call(bf16[1024,4096]{1,0:T(8,128)(2,1)} %refs_0_.1, bf16[32,128]{1,0:T(8,128)(2,1)} %bitcast.12, bf16[512,512]{1,0:T(8,128)(2,1)} %refs_2_.1, bf16[512,512]{1,0:T(8,128)(2,1)} %refs_3_.1, bf16[512,512]{1,0:T(8,128)(2,1)} %refs_4_.1, bf16[512,512]{1,0:T(8,128)(2,1)} %refs_5_.1, ...), custom_call_target="tpu_custom_call" | custom-call | tf_op jit(solution)/shard_map/pallas_call | solution.py:933
  257.9 3.1 %copy.20 = bf16[256,4096]{1,0:T(8,128)(2,1)} copy(bf16[256,4096]{1,0:T(8,128)(2,1)} %shard_map.172) | data formatting | bytes 4194304
